TPU v7x, 256 devices: a whole 4x4x8 slice. The times are simulated.
256 devices in a mesh: ep: 64 (over z, y, core), tp: 4 (over x).
Axes of the slice: x: 4, y: 4, z: 8, core: 2. Of those that a mesh axis runs over, the one named last changes fastest.
Arguments:
- tokens: bfloat16 [49152, 2048], P('ep', 'tp')
- norm_gain: float32 [2048], P('tp'), may hold values from 0.1 to 1.9
- routing: int32 [49152, 2], P('ep'), may hold values from 0 to 63, as said below
- route_weight: float32 [49152, 2], P('ep'), may hold values from 0.2 to 1
- w_gate: bfloat16 [64, 2048, 512], P('ep', 'tp'), may hold values from -0.125 to 0.125
- w_up: bfloat16 [64, 2048, 512], P('ep', 'tp'), may hold values from -0.125 to 0.125
- w_down: bfloat16 [64, 512, 2048], P('ep', None, 'tp'), may hold values from -0.25 to 0.25
- w_branch_in: bfloat16 [2048, 1024], P('ep', 'tp'), may hold values from -0.125 to 0.125
- w_branch_out: bfloat16 [1024, 2048], P('tp', 'ep'), may hold values from -0.1875 to 0.1875
- branch_gate: float32 [2048], P('tp'), may hold values from -3 to 3
Outputs:
- mixed: bfloat16 [49152, 2048], P('ep', 'tp')
Inputs may be any that keep to these rules, and one draw needn't show every extreme that they name: `routing`: each row names two different experts of the same group; expert e belongs to group e // 16. Among the rows of one device (aligned blocks of 768 rows) no expert is named more than 48 times, and in every block all experts of one group are named exactly 48 times.
All inputs are finite; a program needn't handle non-finite values.
Results may differ from a plain program's by a relative error of at most 0.0069.
Values may be sent and summed in bfloat16 or wider, within the bound.
A program may use at most 128 MiB of HBM per device.

v0:
```python
import jax
import jax.numpy as jnp
from jax import lax
from jax.sharding import PartitionSpec as P

GROUPS = 4


epsilon = 1e-06


def sent_to_all(value, axis):
    size = lax.axis_size(axis)
    return lax.all_to_all(
        jnp.broadcast_to(value[None], (size, *value.shape)), axis, 0, 0, tiled=True
    )


def taken_together(value, axis):
    return sent_to_all(value, axis).sum(axis=0)


def gather_turned(arrays, axis, dims):
    turned = [jnp.moveaxis(a, dim, 0) for a, dim in zip(arrays, dims)]
    both = jnp.concatenate([t.reshape(len(t), -1) for t in turned], axis=1)
    filled, at, gathered = (lax.all_gather(both, axis, axis=0, tiled=True), 0, [])
    for t, dim in zip(turned, dims):
        share = filled[:, at : at + t[0].size].reshape(-1, *t.shape[1:])
        gathered.append(jnp.moveaxis(share, 0, dim))
        at += t[0].size
    return tuple(gathered)


def send_back(result):
    return lax.all_to_all(result, "ep", split_axis=0, concat_axis=0, tiled=True)


def body(
    tokens,
    norm_gain,
    routing,
    route_weight,
    w_gate,
    w_up,
    w_down,
    w_branch_in,
    w_branch_out,
    branch_gate,
):
    token_count, quarter = tokens.shape
    full_width = quarter * lax.axis_size("tp")
    floats = tokens.astype(jnp.float32)
    squares = taken_together(jnp.sum(floats * floats, axis=1), "tp")
    normed = (floats * lax.rsqrt(squares[:, None] / full_width + epsilon) * norm_gain).astype(
        jnp.bfloat16
    )
    expert_count = lax.axis_size("ep") * w_gate.shape[0]
    capacity = token_count // (expert_count // GROUPS)
    flat_ids = routing.reshape(-1)
    one_hot = (flat_ids[:, None] == jnp.arange(expert_count, dtype=jnp.int32)[None, :]).astype(
        jnp.int32
    )
    before = jnp.cumsum(one_hot, axis=0) - one_hot
    position = flat_ids * capacity + jnp.sum(before * one_hot, axis=1)
    copies = jnp.repeat(normed, 2, axis=0)
    buffer = jnp.zeros((expert_count * capacity, quarter), jnp.bfloat16).at[position].set(copies)
    buffer = buffer.reshape(expert_count, capacity, quarter)
    gate_whole, up_whole, down_whole = (
        lax.all_gather(w_gate[0], "tp", axis=0, tiled=True),
        lax.all_gather(w_up[0], "tp", axis=0, tiled=True),
        lax.all_gather(w_down[0], "tp", axis=1, tiled=True),
    )
    row_split = lax.all_to_all(
        lax.all_to_all(buffer, "ep", split_axis=0, concat_axis=0, tiled=True),
        "tp",
        split_axis=0,
        concat_axis=2,
        tiled=True,
    )
    slot_rows = row_split.reshape(-1, row_split.shape[2])
    gate_sum = jnp.dot(slot_rows, gate_whole, preferred_element_type=jnp.float32)
    up_sum = jnp.dot(slot_rows, up_whole, preferred_element_type=jnp.float32)
    hidden = (jax.nn.silu(gate_sum) * up_sum).astype(jnp.bfloat16)
    result = jnp.dot(hidden, down_whole, preferred_element_type=jnp.float32).astype(jnp.bfloat16)
    feature_split = lax.all_to_all(
        result.reshape(row_split.shape), "tp", split_axis=2, concat_axis=0, tiled=True
    )
    returned = send_back(feature_split)
    picked = returned.reshape(expert_count * capacity, quarter)[position].reshape(
        token_count, 2, quarter
    )
    routed = jnp.sum(picked.astype(jnp.float32) * route_weight[:, :, None], axis=1)
    branch_tokens = lax.all_to_all(normed, "tp", split_axis=0, concat_axis=1, tiled=True)
    in_cols, out_rows = gather_turned((w_branch_in, w_branch_out), "tp", (1, 0))
    in_whole, out_whole = gather_turned((in_cols, out_rows), "ep", (0, 1))
    branch_hidden = jax.nn.silu(
        jnp.dot(branch_tokens, in_whole, preferred_element_type=jnp.float32)
    ).astype(jnp.bfloat16)
    branch_local = jnp.dot(branch_hidden, out_whole, preferred_element_type=jnp.float32).astype(
        jnp.bfloat16
    )
    branch = lax.all_to_all(branch_local, "tp", split_axis=1, concat_axis=0, tiled=True)
    return (routed + jax.nn.sigmoid(branch_gate) * branch.astype(jnp.float32)).astype(jnp.bfloat16)


def solution(mesh):
    return jax.shard_map(
        body,
        mesh=mesh,
        in_specs=(
            P("ep", "tp"),
            P("tp"),
            P("ep", None),
            P("ep", None),
            P("ep", "tp", None),
            P("ep", "tp", None),
            P("ep", None, "tp"),
            P("ep", "tp"),
            P("tp", "ep"),
            P("tp"),
        ),
        out_specs=P("ep", "tp"),
        check_vma=False,
    )
```

profile of v0, /device:TPU:32, one launch (start us, length us, event | category | flops | bytes accessed | tf_op | source)
XLA Modules:
  0.0 389.8 jit_solution(14819414351238019944)
XLA Ops:
  6.5 0.7 all-gather.10.cloned.1.call-update
  8.0 1.4 fusion.12
  10.0 4.3 %all-to-all-start = ((f32[4,1,768]{2,1,0:T(1,128)}), f32[4,1,768]{2,1,0:T(1,128)S(1)}, u32[]{:S(2)}, u32[]{:S(2)}) async-start(f32[4,1,768]{2,1,0:T(1,128)} %broadcast_in_dim.7), calls=%async_computation | async-start | bytes 24576 | tf_op jit(solution)/shard_map/all_to_all | solution.py:14
  14.3 0.7 all-gather.14.cloned.1.call-update
  15.7 18.1 %reduce-window.6 = s32[64,12,128]{2,1,0:T(8,128)S(1)} reduce-window(s32[64,12,128]{2,1,0:T(8,128)S(1)} %fusion.27, s32[]{:T(128)} %constant.6.clone.1), window={size=1x1x128 pad=0_0x0_0x127_0}, to_apply=%region_0.0 | reduce-window | flops 12484608 | bytes 786436 | tf_op jit(solution)/shard_map/reduce-window
  35.7 0.9 copy-done
  36.5 0.8 broadcast_in_dim.8
  38.0 9.5 %scatter_custom_fusion = bf16[3072,512]{1,0:T(8,128)(2,1)} fusion(s32[1536]{0:T(1024)S(1)} %fusion.32, bf16[1536,512]{1,0:T(8,128)(2,1)S(1)} %reshape.110, bf16[]{:T(256)} %constant.8.clone.1), kind=kCustom, calls=%fused_computation.23 | custom fusion | bytes 3145730 | tf_op jit(solution)/shard_map/scatter | solution.py:66
  47.5 11.9 %all-to-all-start.1 = ((bf16[64,48,512]{2,1,0:T(8,128)(2,1)}), bf16[64,48,512]{2,1,0:T(8,128)(2,1)S(1)}, u32[]{:S(2)}, u32[]{:S(2)}) async-start(bf16[64,48,512]{2,1,0:T(8,128)(2,1)} %bitcast.74), calls=%async_computation.1 | async-start | bytes 6291456 | tf_op jit(solution)/shard_map/all_to_all | solution.py:74
  59.5 13.7 %all_gather.18 = bf16[1024,64]{0,1:T(8,128)(2,1)S(1)} all-gather(bf16[256,64]{0,1:T(8,128)(2,1)S(1)} %pad_maximum_fusion.1), channel_id=1, replica_groups=mesh['ep'=64,'tp'=4] {'tp'}, dimensions={0}, use_global_device_ids=true | all-gather | bytes 163840 | tf_op jit(solution)/shard_map/all_gather | solution.py:26
  73.9 58.3 %all-to-all-done.1 = bf16[64,48,512]{2,1,0:T(8,128)(2,1)S(1)} async-done(((bf16[64,48,512]{2,1,0:T(8,128)(2,1)}), bf16[64,48,512]{2,1,0:T(8,128)(2,1)S(1)}, u32[]{:S(2)}, u32[]{:S(2)}) %all-to-all-start.1) | async-done | bytes 3145760 | tf_op jit(solution)/shard_map/all_to_all | solution.py:74
  132.3 42.1 %all_to_all.81 = bf16[64,48,512]{2,1,0:T(8,128)(2,1)S(1)} all-to-all(bf16[64,48,512]{2,1,0:T(8,128)(2,1)S(1)} %all-to-all-done.1), channel_id=1, replica_groups=mesh['ep'=64,'tp'=4] {'tp'}, dimensions={0} | all-to-all | bytes 6291456 | tf_op jit(solution)/shard_map/all_to_all | solution.py:73
  174.3 2.6 copy.61
  177.0 1.0 copy.71
  178.0 4.8 %fusion.10 = f32[768,512]{1,0:T(8,128)} fusion(bf16[768,2048]{1,0:T(8,128)(2,1)S(1)} %bitcast.79, bf16[1,2048,512]{2,1,0:T(8,128)(2,1)} %all-gather.10.cloned.1.call-done), kind=kOutput, calls=%fused_computation.12 | convolution fusion | flops 1610612736 | bytes 6815744 | tf_op jit(solution)/shard_map/dot_general | solution.py:81
  182.8 8.0 %convolution_convert_fusion = bf16[768,2048]{1,0:T(8,128)(2,1)} fusion(bf16[1,512,2048]{2,1,0:T(8,128)(2,1)} %all-gather.14.cloned.1.call-done, f32[768,512]{1,0:T(8,128)} %fusion.10, bf16[768,2048]{1,0:T(8,128)(2,1)S(1)} %bitcast.80, bf16[1,2048,512]{2,1,0:T(8,128)(2,1)} %all-gather.12.cloned.1.call-done), kind=kOutput, calls=%fused_computation.6 | convolution fusion | flops 3225157632 | bytes 12058624 | tf_op jit(solution)/shard_map/dot_general | solution.py:84
  190.8 10.5 %copy.62 = bf16[16,48,2048]{1,0,2:T(8,128)(2,1)} copy(bf16[16,48,2048]{2,1,0:T(8,128)(2,1)} %bitcast.82) | data formatting | bytes 6291456 | tf_op jit(solution)/shard_map/reshape | solution.py:86
  201.3 14.8 %reshape.120 = bf16[4,2,196608]{2,1,0:T(2,128)(2,1)} reshape(bf16[2048,16,48]{2,1,0:T(8,128)(2,1)} %bitcast.72) | data formatting | bytes 6291456
  216.1 40.3 %all_to_all.82 = bf16[4,2,196608]{2,1,0:T(2,128)(2,1)S(1)} all-to-all(bf16[4,2,196608]{2,1,0:T(2,128)(2,1)} %reshape.120), channel_id=1, replica_groups=mesh['ep'=64,'tp'=4] {'tp'}, dimensions={0} | all-to-all | bytes 6291456 | tf_op jit(solution)/shard_map/all_to_all | solution.py:85
  256.4 4.4 %all-to-all-start.5 = ((bf16[4,192,512]{2,1,0:T(8,128)(2,1)}), bf16[4,192,512]{2,1,0:T(8,128)(2,1)}, u32[]{:S(2)}, u32[]{:S(2)}) async-start(bf16[4,192,512]{2,1,0:T(8,128)(2,1)} %bitcast.78), calls=%async_computation.5 | async-start | bytes 1572864 | tf_op jit(solution)/shard_map/all_to_all | solution.py:93
  260.8 9.9 %reshape.121 = bf16[2048,16,48]{2,1,0:T(8,128)(2,1)} reshape(bf16[4,2,196608]{2,1,0:T(2,128)(2,1)S(1)} %all_to_all.82) | data formatting | bytes 6291456
  270.7 9.5 %copy.63 = bf16[4,16,48,512]{3,2,1,0:T(8,128)(2,1)} copy(bf16[4,16,48,512]{2,1,3,0:T(8,128)(2,1)} %bitcast.73) | data formatting | bytes 6291456 | tf_op jit(solution)/shard_map/all_to_all | solution.py:85
  280.2 7.4 %all-to-all-start.4 = ((bf16[64,48,512]{2,1,0:T(8,128)(2,1)}), bf16[64,48,512]{2,1,0:T(8,128)(2,1)S(1)}, u32[]{:S(2)}, u32[]{:S(2)}) async-start(bf16[64,48,512]{2,1,0:T(8,128)(2,1)} %bitcast.77), calls=%async_computation.4 | async-start | bytes 6291456 | tf_op jit(solution)/shard_map/all_to_all | solution.py:35
  287.7 2.1 copy.69
  289.8 7.0 %fusion.4 = bf16[192,2048]{1,0:T(8,128)(2,1)} fusion(bf16[2048,2048]{1,0:T(8,128)(2,1)} %all-gather.8.cloned.1.call-done, bf16[192,2048]{1,0:T(8,128)(2,1)} %bitcast.84), kind=kOutput, calls=%fused_computation.8 | convolution fusion | flops 1611988992 | bytes 9961472 | tf_op jit(solution)/shard_map/dot_general | solution.py:99
  296.8 2.1 copy.74
  298.9 61.6 %all-to-all-done.4 = bf16[64,48,512]{2,1,0:T(8,128)(2,1)S(1)} async-done(((bf16[64,48,512]{2,1,0:T(8,128)(2,1)}), bf16[64,48,512]{2,1,0:T(8,128)(2,1)S(1)}, u32[]{:S(2)}, u32[]{:S(2)}) %all-to-all-start.4) | async-done | bytes 3145760 | tf_op jit(solution)/shard_map/all_to_all | solution.py:35
  360.5 4.5 %all-to-all-start.6 = ((bf16[192,4,512]{2,0,1:T(8,128)(2,1)}), bf16[192,4,512]{2,0,1:T(8,128)(2,1)}, u32[]{:S(2)}, u32[]{:S(2)}) async-start(bf16[192,4,512]{2,0,1:T(8,128)(2,1)} %bitcast.81), calls=%async_computation.6 | async-start | bytes 1572864 | tf_op jit(solution)/shard_map/all_to_all | solution.py:102
  365.8 5.4 %gather_fusion = bf16[1536,512]{1,0:T(8,128)(2,1)} fusion(bf16[3072,512]{1,0:T(8,128)(2,1)S(1)} %bitcast.71, s32[2048]{0:T(1024)S(1)} %pad_clamp_fusion), kind=kCustom, calls=%fused_computation | custom fusion | bytes 3151872 | tf_op jit(solution)/shard_map/gather | solution.py:89
  371.2 3.4 reshape.96
  374.6 5.9 %multiply_reduce_fusion = f32[768,512]{1,0:T(8,128)} fusion(f32[768,2,512]{2,1,0:T(2,128)S(1)} %reshape.96, f32[768,2]{1,0:T(8,128)S(1)} %copy.64), kind=kLoop, calls=%fused_computation.7 | loop fusion | flops 1179648 | bytes 4724736 | tf_op jit(solution)/shard_map/reduce_sum | solution.py:92
  380.6 2.7 fusion.16
  (55 shorter events, 6.0 us)
Async XLA Ops:
  6.5 8.5 %copy-start.2 = (s32[768,2]{0,1:T(2,128)S(1)}, s32[768,2]{0,1:T(2,128)}, u32[]{:S(2)}) copy-start(s32[768,2]{0,1:T(2,128)} %param.12) | copy-start | bytes 18436
  6.5 171.5 %all-gather.10.cloned.1.call-start = ((), (), s32[]{:S(2)}) async-start(), calls=%async_computation.8 | async-start | bytes 2621440 | tf_op jit(solution)/shard_map/all_gather | solution.py:69
  7.3 175.5 %all-gather.12.cloned.1.call-start = ((), (), s32[]{:S(2)}) async-start(), calls=%async_computation.9 | async-start | bytes 2621440 | tf_op jit(solution)/shard_map/all_gather | solution.py:70
  10.0 25.4 %all-to-all-start = ((f32[4,1,768]{2,1,0:T(1,128)}), f32[4,1,768]{2,1,0:T(1,128)S(1)}, u32[]{:S(2)}, u32[]{:S(2)}) async-start(f32[4,1,768]{2,1,0:T(1,128)} %broadcast_in_dim.7), calls=%async_computation | async-start | bytes 24576 | tf_op jit(solution)/shard_map/all_to_all | solution.py:14
  14.3 168.5 %all-gather.14.cloned.1.call-start = ((), (), s32[]{:S(2)}) async-start(), calls=%async_computation.10 | async-start | bytes 2621440 | tf_op jit(solution)/shard_map/all_gather | solution.py:71
  33.8 1.6 copy-start.1
  33.8 1.6 copy-start.7
  35.6 0.9 copy-start
  47.5 12.0 %copy-start.3 = (bf16[256,32]{0,1:T(8,128)(2,1)S(1)}, bf16[256,32]{0,1:T(8,128)(2,1)}, u32[]{:S(2)}) copy-start(bf16[256,32]{0,1:T(8,128)(2,1)} %param.18) | copy-start | bytes 49156
  47.5 12.0 %copy-start.4 = (bf16[32,256]{1,0:T(8,128)(2,1)S(1)}, bf16[32,256]{1,0:T(8,128)(2,1)}, u32[]{:S(2)}) copy-start(bf16[32,256]{1,0:T(8,128)(2,1)} %param.17) | copy-start | bytes 49156
  47.5 84.7 %all-to-all-start.1 = ((bf16[64,48,512]{2,1,0:T(8,128)(2,1)}), bf16[64,48,512]{2,1,0:T(8,128)(2,1)S(1)}, u32[]{:S(2)}, u32[]{:S(2)}) async-start(bf16[64,48,512]{2,1,0:T(8,128)(2,1)} %bitcast.74), calls=%async_computation.1 | async-start | bytes 6291456 | tf_op jit(solution)/shard_map/all_to_all | solution.py:74
  59.4 230.4 %all-gather.8.cloned.1.call-start = ((), (), s32[]{:S(2)}) async-start(), calls=%async_computation.7 | async-start | bytes 8519680 | tf_op jit(solution)/shard_map/all_gather | solution.py:26
  256.4 23.9 %all-to-all-start.5 = ((bf16[4,192,512]{2,1,0:T(8,128)(2,1)}), bf16[4,192,512]{2,1,0:T(8,128)(2,1)}, u32[]{:S(2)}, u32[]{:S(2)}) async-start(bf16[4,192,512]{2,1,0:T(8,128)(2,1)} %bitcast.78), calls=%async_computation.5 | async-start | bytes 1572864 | tf_op jit(solution)/shard_map/all_to_all | solution.py:93
  280.2 80.3 %all-to-all-start.4 = ((bf16[64,48,512]{2,1,0:T(8,128)(2,1)}), bf16[64,48,512]{2,1,0:T(8,128)(2,1)S(1)}, u32[]{:S(2)}, u32[]{:S(2)}) async-start(bf16[64,48,512]{2,1,0:T(8,128)(2,1)} %bitcast.77), calls=%async_computation.4 | async-start | bytes 6291456 | tf_op jit(solution)/shard_map/all_to_all | solution.py:35
  296.8 68.2 %copy-start.8 = (f32[512]{0:T(512)S(1)}, f32[512]{0:T(512)}, u32[]{:S(2)}) copy-start(f32[512]{0:T(512)} %param.19) | copy-start | bytes 6148
  296.8 68.8 %copy-start.6 = (f32[768,2]{0,1:T(2,128)S(1)}, f32[768,2]{0,1:T(2,128)}, u32[]{:S(2)}) copy-start(f32[768,2]{0,1:T(2,128)} %param.13) | copy-start | bytes 18436
  360.5 20.0 %all-to-all-start.6 = ((bf16[192,4,512]{2,0,1:T(8,128)(2,1)}), bf16[192,4,512]{2,0,1:T(8,128)(2,1)}, u32[]{:S(2)}, u32[]{:S(2)}) async-start(bf16[192,4,512]{2,0,1:T(8,128)(2,1)} %bitcast.81), calls=%async_computation.6 | async-start | bytes 1572864 | tf_op jit(solution)/shard_map/all_to_all | solution.py:102
  374.6 5.9 %copy-start.5 = (f32[512]{0:T(512)S(1)}, f32[512]{0:T(512)}, u32[]{:S(2)}) copy-start(f32[512]{0:T(512)} %add_divide_fusion) | copy-start | bytes 6148
Sparse Core Ops, SparseCore 0:
  9.1 35.9 all-gather.9
  46.9 34.3 all-gather.11
  83.2 33.3 all-gather.13
  119.2 82.6 all-gather.7
where the time goes:
time: 393 us; the launch traced here: 390 us
  waiting for transfers between devices  122 us (31%)
  blocking collectives  96.1 us (24%)
  local copies, waits for them, and re-layouts  75.7 us (19%)
  starting transfers between devices  32.6 us (8%)
  other arithmetic  30.1 us (8%)
  matrix products  19.8 us (5%)
  between operations  13.4 us (3%)
    all_to_all x1, waiting for transfers between devices, send_back(): return lax.all_to_all(result, 'ep', split_axis=0, concat_axis=0, tiled=True)  61.6 us
    all_to_all x1, waiting for transfers between devices, body(): lax.all_to_all(buffer, 'ep', split_axis=0, concat_axis=0, tiled=True)  58.3 us
    all_to_all x1, blocking collectives, body(): lax.all_to_all(lax.all_to_all(buffer, 'ep', split_axis=0, concat_axis=0,...  42.1 us
    all_to_all x1, blocking collectives, body(): lax.all_to_all(result.reshape(row_split.shape), 'tp', split_axis=2, conca...  40.3 us
    unnamed x23, local copies, waits for them, and re-layouts  27 us
    another operation x3, other arithmetic  18.4 us
    all_gather x1, blocking collectives, gather_turned(): lax.all_gather(both, axis, axis=0, tiled=True)  13.7 us
    all_to_all x1, starting transfers between devices, body(): lax.all_to_all(buffer, 'ep', split_axis=0, concat_axis=0, tiled=True)  11.9 us
  transfers between devices with their start and end apart: 9, of which 2 were waited for; matrix products, arithmetic and copies ran while one was open for 31% of the time, Pallas kernels for 0%

commit v1 on v0

v1 whole, which is shorter than its diff:
```python
import functools

import jax
import jax.numpy as jnp
from jax import lax
from jax.experimental import pallas as pl
from jax.experimental.pallas import tpu as pltpu
from jax.sharding import PartitionSpec as P

EPSILON = 1e-06
MESH = pl.DeviceIdType.MESH
CAP = 48
F = 512
T = 768
NQ = 16
BLK = 4 * CAP


def kernel(
    tok_hbm, gain_hbm, rout_t, rout, rw, wg_hbm, wu_hbm, wd_hbm, bw_hbm, gate_ref,
    out_ref,
    tok, gains, send, land, weights, bw, normed, hidden, result, ret, btok, bnorm, bhid, bres, bret, acc,
    lsem, gsend, grecv, btsend, btrecv, brsend, brrecv, zsend, zrecv, xsend, xrecv, ysend, yrecv, dsend, drecv,
    wsend, wrecv, fsend, frecv, esend, erecv, rsend, rrecv,
):
    ep = lax.axis_index("ep")
    x = lax.axis_index("tp")
    z, y, c = ep // 8, (ep // 2) % 4, ep % 2
    m_own, s4 = ep // 4, ep % 4
    is_self = x == (2 * ep) % 4
    sigma = (x - s4 + 4) % 4

    def remote(src, dst, ssem, rsem, e, xx):
        return pltpu.make_async_remote_copy(
            src_ref=src, dst_ref=dst, send_sem=ssem, recv_sem=rsem,
            device_id={"ep": e, "tp": xx}, device_id_type=MESH,
        )

    def lanes(index, width):
        return pl.ds(pl.multiple_of(index * width, width), width)

    def ep_of(zz, yy, cc):
        return (zz * 4 + yy) * 2 + cc

    loads = [
        pltpu.make_async_copy(tok_hbm, tok, lsem.at[0]),
        pltpu.make_async_copy(bw_hbm, bw.at[:, z, y, c, :, lanes(x, 256)], lsem.at[1]),
        pltpu.make_async_copy(gain_hbm, gains.at[x], lsem.at[2]),
        pltpu.make_async_copy(tok_hbm.at[pl.ds(x * 192, 192), :], btok.at[:, lanes(x, F)], lsem.at[3]),
        pltpu.make_async_copy(wg_hbm, weights.at[0, x], lsem.at[4]),
        pltpu.make_async_copy(wu_hbm, weights.at[1, x], lsem.at[5]),
        pltpu.make_async_copy(wd_hbm, weights.at[2, x], lsem.at[6]),
    ]
    for load in loads:
        load.start()
    for load in loads:
        load.wait()

    def z_copy(d):
        zz = (z + d) % 8
        mine = bw.at[:, z, y, c, :, lanes(x, 256)]
        return remote(mine, mine, zsend.at[d], zrecv.at[d], ep_of(zz, y, c), x)

    for d in range(1, 8):
        z_copy(d).start()

    def gain_copy(d):
        return remote(gains.at[x], gains.at[x], gsend.at[d], grecv.at[d], ep, (x + d) % 4)

    def btok_copy(d):
        xx = (x + d) % 4
        return remote(
            tok.at[pl.ds(xx * 192, 192), :], btok.at[:, lanes(x, F)], btsend.at[d], btrecv.at[d], ep, xx
        )

    for d in range(1, 4):
        gain_copy(d).start()

    experts = lax.broadcasted_iota(jnp.int32, (64, T), 0)
    r0, r1 = rout_t[0:1, :], rout_t[1:2, :]
    named0, named1 = experts == r0, experts == r1
    one_hot = jnp.where(named0 | named1, 1.0, 0.0).astype(jnp.bfloat16)
    earlier = jnp.where(
        lax.broadcasted_iota(jnp.int32, (T, T), 0) < lax.broadcasted_iota(jnp.int32, (T, T), 1), 1.0, 0.0
    ).astype(jnp.bfloat16)
    before = jnp.dot(one_hot, earlier, preferred_element_type=jnp.float32)
    slot0 = r0 * CAP + jnp.sum(jnp.where(named0, before, 0.0), axis=0, keepdims=True).astype(jnp.int32)
    slot1 = r1 * CAP + jnp.sum(jnp.where(named1, before, 0.0), axis=0, keepdims=True).astype(jnp.int32)

    def block_at(q):
        half = (q + 1) // 2
        return (m_own + 16 + half * (2 * (q % 2) - 1)) % 16

    def dispatch_copy(q, j):
        m, xx = block_at(q), (x + j) % 4
        r = (xx - s4 + 4) % 4
        return remote(
            send.at[m, pl.ds(pl.multiple_of(r * CAP, 16), CAP), :],
            land.at[m_own, :, lanes(x, F)],
            esend.at[q * 4 + j],
            erecv.at[m_own * 4 + x],
            m * 4 + r,
            xx,
        )

    def pack(q, carry):
        m = block_at(q)
        slots = lax.broadcasted_iota(jnp.int32, (BLK, T), 0) + m * BLK
        pick = jnp.where((slots == slot0) | (slots == slot1), 1.0, 0.0).astype(jnp.bfloat16)
        send[m] = jnp.dot(pick, tok[...], preferred_element_type=jnp.float32).astype(jnp.bfloat16)
        for j in range(4):
            if j == 0:
                own = (q == 0) & is_self

                @pl.when(jnp.logical_not(own))
                def _():
                    dispatch_copy(q, j).start()

                @pl.when(own)
                def _():
                    land[m_own, :, lanes(x, F)] = send[m_own, pl.ds(pl.multiple_of(s4 * CAP, 16), CAP), :]
            else:
                dispatch_copy(q, j).start()
        return carry

    lax.fori_loop(0, NQ, pack, 0)

    def w_copy(k, way):
        return remote(
            weights.at[k, x], weights.at[k, x], wsend.at[k, way], wrecv.at[k, way], ep, (x + (1, 3)[way]) % 4
        )

    def f_copy(k, way):
        slot = (x + (3, 1)[way]) % 4
        if k == 2:
            piece = weights.at[2, slot, pl.ds(256 * way, 256), :]
        else:
            piece = weights.at[way, slot]
        return remote(piece, piece, fsend.at[k // 2, way], frecv.at[k // 2, way], ep, (x + (1, 3)[way]) % 4)

    for k in range(3):
        for way in range(2):
            w_copy(k, way).start()
    for d in range(1, 4):
        btok_copy(d).start()

    for d in range(1, 8):
        z_copy(d).wait_recv()

    def x_copy(k, d):
        mine = bw.at[k, :, y, c, :, lanes(x, 256)]
        return remote(mine, mine, xsend.at[k, d], xrecv.at[k, d], ep, (x + d) % 4)

    for d in range(1, 4):
        for k in range(2):
            x_copy(k, d).start()
    for way in range(2):
        for k in range(2):
            w_copy(k, way).wait_recv()
    for way in range(2):
        f_copy(0, way).start()
    for way in range(2):
        w_copy(2, way).wait_recv()
    for way in range(2):
        f_copy(2, way).start()
    for d in range(1, 4):
        for k in range(2):
            x_copy(k, d).wait_recv()

    def y_copy(k, way):
        mine = bw.at[k, :, y, c]
        return remote(mine, mine, ysend.at[k, way], yrecv.at[k, way], ep_of(z, (y + (1, 3)[way]) % 4, c), x)

    def y_forward(way):
        slot = (y + (3, 1)[way]) % 4
        piece = bw.at[way, :, slot, c]
        return remote(piece, piece, ysend.at[2, way], yrecv.at[2, way], ep_of(z, (y + (1, 3)[way]) % 4, c), x)

    for way in range(2):
        for k in range(2):
            y_copy(k, way).start()

    for d in range(1, 4):
        gain_copy(d).wait_recv()
    for way in range(2):
        f_copy(0, way).wait_recv()
    for way in range(2):
        f_copy(2, way).wait_recv()

    def norm_rows(source, target):
        floats = source.astype(jnp.float32)
        squares = jnp.sum(floats * floats, axis=1, keepdims=True)
        scaled = floats * lax.rsqrt(squares * (1.0 / (4 * F)) + EPSILON)
        for k in range(4):
            target[:, k * F : (k + 1) * F] = (scaled[:, k * F : (k + 1) * F] * gains[k, 0:1, :]).astype(jnp.bfloat16)

    def arrival(m, xx):
        there = land.at[m, :, lanes(xx, F)]
        return remote(there, there, esend.at[0], erecv.at[m * 4 + xx], ep, xx)

    def return_copy(jj, m):
        quarter = (x + (0, 1, 3, 2)[jj]) % 4
        return remote(
            result.at[quarter, m], ret.at[ep], rsend.at[jj * 16 + m], rrecv.at[ep], m * 4 + sigma, quarter
        )

    def expert(i, carry):
        part = (z // 2 + i) % 4
        for mm in range(4):
            m = part * 4 + mm
            for xx in range(4):

                @pl.when(jnp.logical_not(is_self & (m == m_own) & (x == xx)))
                def _():
                    arrival(m, xx).wait_recv()

        def one(r, inner):
            m, row = part * 4 + r // 3, pl.multiple_of((r % 3) * 16, 16)
            norm_rows(land[m, pl.ds(row, 16), :], normed.at[pl.ds(pl.multiple_of(r * 16, 16), 16), :])
            return inner

        lax.fori_loop(0, 12, one, 0)
        for n in range(2):
            cols = slice(n * 256, n * 256 + 256)
            sums = []
            for k in range(2):
                total = jnp.dot(normed[:, 0:F], weights[k, 0, :, cols], preferred_element_type=jnp.float32)
                for h in range(1, 4):
                    total += jnp.dot(
                        normed[:, h * F : (h + 1) * F], weights[k, h, :, cols], preferred_element_type=jnp.float32
                    )
                sums.append(total)
            gate_sum, up_sum = sums
            hidden[:, cols] = (gate_sum / (1.0 + jnp.exp(-gate_sum)) * up_sum).astype(jnp.bfloat16)
        for jj in range(4):
            quarter = (x + (0, 1, 3, 2)[jj]) % 4
            rows = jnp.dot(hidden[...], weights[2, quarter], preferred_element_type=jnp.float32)
            result[quarter, pl.ds(part * 4, 4)] = rows.astype(jnp.bfloat16).reshape(4, CAP, F)
            for mm in range(4):
                m = part * 4 + mm
                if jj == 0:
                    own = is_self & (m == m_own)

                    @pl.when(jnp.logical_not(own))
                    def _():
                        return_copy(jj, m).start()

                    @pl.when(own)
                    def _():
                        ret[ep] = result[x, m_own]
                else:
                    return_copy(jj, m).start()
        return carry

    lax.fori_loop(0, 4, expert, 0)

    for way in range(2):
        for k in range(2):
            y_copy(k, way).wait_recv()
    for way in range(2):
        y_forward(way).start()
    for way in range(2):
        y_forward(way).wait_recv()

    def d_copy(k):
        mine = bw.at[k, :, :, c]
        return remote(mine, mine, dsend.at[k], drecv.at[k], ep_of(z, y, 1 - c), x)

    for k in range(2):
        d_copy(k).start()

    for d in range(1, 4):
        btok_copy(d).wait_recv()

    def branch_norm(r, carry):
        rows = pl.ds(pl.multiple_of(r * 16, 16), 16)
        norm_rows(btok[rows, :], bnorm.at[rows, :])
        return carry

    lax.fori_loop(0, 12, branch_norm, 0)

    lane_experts = lax.broadcasted_iota(jnp.int32, (T, 128), 1)
    c0, c1 = rout[:, 0:1], rout[:, 1:2]
    named0, named1 = lane_experts == c0, lane_experts == c1
    one_hot = jnp.where(named0 | named1, 1.0, 0.0).astype(jnp.bfloat16)
    earlier = jnp.where(
        lax.broadcasted_iota(jnp.int32, (T, T), 1) < lax.broadcasted_iota(jnp.int32, (T, T), 0), 1.0, 0.0
    ).astype(jnp.bfloat16)
    before = jnp.dot(earlier, one_hot, preferred_element_type=jnp.float32)
    place0 = c0 * CAP + jnp.sum(jnp.where(named0, before, 0.0), axis=1, keepdims=True).astype(jnp.int32)
    place1 = c1 * CAP + jnp.sum(jnp.where(named1, before, 0.0), axis=1, keepdims=True).astype(jnp.int32)

    for k in range(2):
        d_copy(k).wait_recv()

    w_in = bw.at[0].reshape(2048, 1024)
    w_out = bw.at[1].reshape(2048, 1024)
    for n in range(4):
        cols = slice(n * 256, n * 256 + 256)
        total = jnp.dot(bnorm[...], w_in[:, cols], preferred_element_type=jnp.float32)
        bhid[:, cols] = (total / (1.0 + jnp.exp(-total))).astype(jnp.bfloat16)

    def bret_copy(d):
        xx = (x + d) % 4
        return remote(
            bres.at[xx], bret.at[pl.ds(x * 192, 192), :], brsend.at[d], brrecv.at[d], ep, xx
        )

    for d in (1, 3, 2, 0):
        quarter = (x + d) % 4
        rows = lax.dot_general(
            bhid[...],
            w_out[pl.ds(pl.multiple_of(quarter * F, F), F), :],
            (((1,), (1,)), ((), ())),
            preferred_element_type=jnp.float32,
        )
        if d == 0:
            bret[pl.ds(pl.multiple_of(x * 192, 192), 192), :] = rows.astype(jnp.bfloat16)
        else:
            bres[quarter] = rows.astype(jnp.bfloat16)
            bret_copy(d).start()

    acc[...] = jnp.zeros_like(acc)

    def returned(e):
        return remote(ret.at[e], ret.at[e], rsend.at[0], rrecv.at[e], ep, x)

    def combine(i, carry):
        part = (z // 2 + i) % 4

        def wait(k, inner):
            e = part * 16 + k

            @pl.when(jnp.logical_not(is_self & (e == ep)))
            def _():
                returned(e).wait_recv()

            return inner

        lax.fori_loop(0, 16, wait, 0)
        rows = ret[pl.ds(part * 16, 16)].reshape(16 * CAP, F)
        for h in range(3):
            sl = slice(h * 256, h * 256 + 256)
            slots = lax.broadcasted_iota(jnp.int32, (256, 16 * CAP), 1) + part * (16 * CAP)
            mix = jnp.where(slots == place0[sl], rw[sl, 0:1], 0.0) + jnp.where(slots == place1[sl], rw[sl, 1:2], 0.0)
            acc[sl, :] += jnp.dot(mix.astype(jnp.bfloat16), rows, preferred_element_type=jnp.float32)
        return carry

    lax.fori_loop(0, 4, combine, 0)
    for d in range(1, 4):
        bret_copy(d).wait_recv()
    share = 1.0 / (1.0 + jnp.exp(-gate_ref[0:1, :]))
    for h in range(3):
        sl = slice(h * 256, h * 256 + 256)
        out_ref[sl, :] = (acc[sl, :] + share * bret[sl, :].astype(jnp.float32)).astype(jnp.bfloat16)

    for d in range(1, 8):
        z_copy(d).wait_send()
    for d in range(1, 4):
        gain_copy(d).wait_send()
        btok_copy(d).wait_send()
        bret_copy(d).wait_send()
        for k in range(2):
            x_copy(k, d).wait_send()
    for way in range(2):
        for k in range(3):
            w_copy(k, way).wait_send()
        for k in (0, 2):
            f_copy(k, way).wait_send()
        for k in range(2):
            y_copy(k, way).wait_send()
        y_forward(way).wait_send()
    for k in range(2):
        d_copy(k).wait_send()

    def sent(q, carry):
        for j in range(4):
            if j == 0:

                @pl.when(jnp.logical_not((q == 0) & is_self))
                def _():
                    dispatch_copy(q, j).wait_send()

                @pl.when(jnp.logical_not((q == m_own) & is_self))
                def _():
                    return_copy(j, q).wait_send()
            else:
                dispatch_copy(q, j).wait_send()
                return_copy(j, q).wait_send()
        return carry

    lax.fori_loop(0, NQ, sent, 0)


def body(
    tokens, norm_gain, routing, route_weight, w_gate, w_up, w_down, w_branch_in, w_branch_out, branch_gate
):
    bf16, f32 = jnp.bfloat16, jnp.float32
    vmem = pl.BlockSpec(memory_space=pltpu.VMEM)
    hbm = pl.BlockSpec(memory_space=pl.ANY)
    dma = pltpu.SemaphoreType.DMA
    bw = jnp.stack([w_branch_in, w_branch_out.T])
    return pl.pallas_call(
        kernel,
        out_shape=jax.ShapeDtypeStruct((T, F), bf16),
        in_specs=[hbm, hbm, vmem, vmem, vmem, hbm, hbm, hbm, hbm, vmem],
        out_specs=vmem,
        scratch_shapes=[
            pltpu.VMEM((T, F), bf16),
            pltpu.VMEM((4, 8, F), f32),
            pltpu.VMEM((NQ, BLK, F), bf16),
            pltpu.VMEM((NQ, CAP, 4 * F), bf16),
            pltpu.VMEM((3, 4, 512, 512), bf16),
            pltpu.VMEM((2, 8, 4, 2, 32, 1024), bf16),
            pltpu.VMEM((BLK, 4 * F), bf16),
            pltpu.VMEM((BLK, 512), bf16),
            pltpu.VMEM((4, NQ, CAP, F), bf16),
            pltpu.VMEM((64, CAP, F), bf16),
            pltpu.VMEM((192, 4 * F), bf16),
            pltpu.VMEM((192, 4 * F), bf16),
            pltpu.VMEM((192, 1024), bf16),
            pltpu.VMEM((4, 192, F), bf16),
            pltpu.VMEM((T, F), bf16),
            pltpu.VMEM((T, F), f32),
            dma((7,)),
            dma((4,)), dma((4,)),
            dma((4,)), dma((4,)),
            dma((4,)), dma((4,)),
            dma((8,)), dma((8,)),
            dma((2, 4)), dma((2, 4)),
            dma((3, 2)), dma((3, 2)),
            dma((2,)), dma((2,)),
            dma((3, 2)), dma((3, 2)),
            dma((2, 2)), dma((2, 2)),
            dma((64,)), dma((64,)),
            dma((64,)), dma((64,)),
        ],
        compiler_params=pltpu.CompilerParams(has_side_effects=True, vmem_limit_bytes=60 * 1024 * 1024),
        name="layer",
    )(
        tokens,
        jnp.broadcast_to(norm_gain[None, :], (8, F)),
        routing.T,
        routing,
        route_weight,
        w_gate[0],
        w_up[0],
        w_down[0],
        bw,
        jnp.broadcast_to(branch_gate[None, :], (8, F)),
    )


def solution(mesh):
    return jax.shard_map(
        body,
        mesh=mesh,
        in_specs=(
            P("ep", "tp"),
            P("tp"),
            P("ep", None),
            P("ep", None),
            P("ep", "tp", None),
            P("ep", "tp", None),
            P("ep", None, "tp"),
            P("ep", "tp"),
            P("tp", "ep"),
            P("tp"),
        ),
        out_specs=P("ep", "tp"),
        check_vma=False,
    )
```

time: 393 us -> 224 us (0.57)
  Pallas kernels: 0 us -> 216 us
  waiting for transfers between devices: 122 us -> 0 us
  blocking collectives: 96.1 us -> 0 us
  local copies, waits for them, and re-layouts: 75.7 us -> 5.92 us
  starting transfers between devices: 32.6 us -> 0 us
  other arithmetic: 30.1 us -> 0.61 us
  matrix products: 19.8 us -> 0 us
  between operations: 13.4 us -> 0.02 us
    pallas_call x0 -> x1, Pallas kernels: none -> 216 us  [body(): pl.pallas_call(kernel, out_shape=jax.ShapeDtypeStruct((T, F), bf16), in_s...]
    all_to_all x5 -> x0, waiting for transfers between devices: 120 us -> none  [the longest x1 61.6 us: send_back(): return lax.all_to_all(result, 'ep', split_axis=0, concat_axis=0, tiled=True)]
    all_to_all x2 -> x0, blocking collectives: 82.4 us -> none  [the longest x1 42.1 us: body(): lax.all_to_all(lax.all_to_all(buffer, 'ep', split_axis=0, concat_axis=0,...]
    all_to_all x5 -> x0, starting transfers between devices: 32.5 us -> none  [the longest x1 11.9 us: body(): lax.all_to_all(buffer, 'ep', split_axis=0, concat_axis=0, tiled=True)]
    unnamed x23 -> x15, local copies, waits for them, and re-layouts: 27 us -> 4.72 us
    dot_general x3 -> x0, matrix products: 19.8 us -> none  [the longest x1 8 us: body(): jnp.dot(hidden, down_whole, preferred_element_type=jnp.float32)]
    another operation x3 -> x1, other arithmetic: 18.4 us -> 0.61 us  [body(): bw = jnp.stack([w_branch_in, w_branch_out.T])]
    all_to_all x4 -> x0, local copies, waits for them, and re-layouts: 16.4 us -> none  [the longest x1 9.54 us: body(): lax.all_to_all(result.reshape(row_split.shape), 'tp', split_axis=2, conca...]
  transfers between devices with their start and end apart: 9 -> 0, of which waited for: 2 -> 0; matrix products, arithmetic and copies ran while one was open for 31% -> 0% of each run, Pallas kernels for 0% -> 0%
where the time goes in v1:
time: 224 us; the launch traced here: 222 us
  Pallas kernels  216 us (96%)
  local copies, waits for them, and re-layouts  5.92 us (3%)
    pallas_call x1, Pallas kernels, body(): pl.pallas_call(kernel, out_shape=jax.ShapeDtypeStruct((T, F), bf16), in_s...  216 us
    unnamed x15, local copies, waits for them, and re-layouts  4.72 us

profile of v1, /device:TPU:32, one launch (start us, length us, event | category | flops | bytes accessed | tf_op | source)
XLA Modules:
  0.0 222.3 jit_solution(2052846537183041472)
XLA Ops:
  0.0 0.0 copy-start.4
  0.0 0.0 copy-start.5
  0.0 0.7 copy-done.4
  0.7 0.0 copy-start.1
  0.7 0.0 copy-start.2
  0.7 0.6 broadcast_in_dim.4.gain_hbm
  1.3 0.0 copy-done.5
  1.3 0.6 broadcast_in_dim.5.gate_ref
  1.9 0.0 copy-done.1
  1.9 0.0 copy-done.2
  1.9 0.0 copy-start.3
  1.9 0.6 pad_maximum_fusion.bw_hbm
  2.5 0.1 copy-done.3
  2.6 0.0 copy-start
  2.6 0.9 copy.12.rw
  3.5 0.0 copy-done
  3.5 0.9 copy.11.rout
  4.5 215.7 %layer.1 = bf16[768,512]{1,0:T(8,128)(2,1)} custom-call(bf16[768,512]{1,0:T(8,128)(2,1)} %tok_hbm.1, f32[8,512]{1,0:T(8,128)} %broadcast_in_dim.4.gain_hbm, s32[2,768]{1,0:T(2,128)} %bitcast.11, s32[768,2]{1,0:T(8,128)} %copy.11.rout, f32[768,2]{1,0:T(8,128)} %copy.12.rw, bf16[512,512]{1,0:T(8,128)(2,1)} %bitcast.8, bf16[512,512]{1,0:T(8,128)(2,1)} %bitcast.9, ...), custom_call_target="tpu_custom_call" | custom-call | tf_op jit(solution)/shard_map/layer/pallas_call | solution.py:403
  220.2 2.1 copy.14
Async XLA Ops:
  0.0 0.7 copy-start.4
  0.0 1.3 copy-start.5
  0.7 1.2 copy-start.1
  0.7 1.2 copy-start.2
  1.9 0.7 copy-start.3
  2.6 0.9 copy-start

commit v2 on v1

v2 whole, which is shorter than its diff:
```python
import functools

import jax
import jax.numpy as jnp
from jax import lax
from jax.experimental import pallas as pl
from jax.experimental.pallas import tpu as pltpu
from jax.sharding import PartitionSpec as P

EPSILON = 1e-06
MESH = pl.DeviceIdType.MESH
CAP = 48
F = 512
T = 768
NQ = 16
BLK = 4 * CAP
EARLY = 14
FIRST = 4


def kernel(
    tok_hbm, gain_hbm, rout_t, rw_t, wg_hbm, wu_hbm, wd_hbm, bwi_hbm, bwo_hbm, gate_ref,
    out_ref,
    tok, gains, send, land, weights, bw, normed, hidden, result, ret, btok, bnorm, bhid, bres, bret, acc, slots_v,
    lsem, gsend, grecv, btsend, btrecv, brsend, brrecv, zsend, zrecv, xsend, xrecv, ysend, yrecv, dsend, drecv,
    wsend, wrecv, fsend, csend, esend, erecv, rsend, rrecv,
):
    ep = lax.axis_index("ep")
    x = lax.axis_index("tp")
    z, y, c = ep // 8, (ep // 2) % 4, ep % 2
    m_own, s4 = ep // 4, ep % 4
    served = (ep // 2) * 2 + x // 2
    sigma = ((x % 2) * 2 + c - served % 4 + 4) % 4
    is_self = sigma == s4
    primary = x // 2 == c
    rel = (x - 2 * c + 4) % 4

    def remote(src, dst, ssem, rsem, e, xx):
        return pltpu.make_async_remote_copy(
            src_ref=src, dst_ref=dst, send_sem=ssem, recv_sem=rsem,
            device_id={"ep": e, "tp": xx}, device_id_type=MESH,
        )

    def lanes(index, width):
        return pl.ds(pl.multiple_of(index * width, width), width)

    def ep_of(zz, yy, cc):
        return (zz * 4 + yy) * 2 + cc

    def block_at(q):
        half = (q + 1) // 2
        return (m_own + 16 + half * (2 * (q % 2) - 1)) % 16

    def target_of(m, j):
        xx = (x + j) % 4
        h = 2 * (xx % 2) + (s4 + xx // 2) % 2
        r = (h - s4 + 4) % 4
        return r, m * 4 + 2 * (r // 2) + h % 2, xx

    barrier = pltpu.get_barrier_semaphore()

    def greet_one(e, xx):
        pl.semaphore_signal(barrier, inc=1, device_id={"ep": e, "tp": xx}, device_id_type=MESH)

    for d in range(1, 8):
        greet_one(ep_of((z + d) % 8, y, c), x)
    for d in range(1, 4):
        greet_one(ep, (x + d) % 4)
    for d in (1, 3):
        greet_one(ep_of(z, (y + d) % 4, c), x)
    greet_one(ep_of(z, y, 1 - c), x)

    def greet(m, carry):
        for j in range(4):
            _, e, xx = target_of(m, j)

            @pl.when(jnp.logical_not((e == ep) & (xx == x)))
            def _():
                greet_one(e, xx)

            @pl.when(jnp.logical_not(is_self & (m == m_own) & (j == 0)))
            def _():
                greet_one(m * 4 + sigma, xx)
        return carry

    lax.fori_loop(0, NQ, greet, 0)

    loads = [
        pltpu.make_async_copy(tok_hbm, tok, lsem.at[0]),
        pltpu.make_async_copy(bwi_hbm, bw.at[0, z, y, c, :, lanes(x, 256)], lsem.at[1]),
        pltpu.make_async_copy(bwo_hbm, bw.at[1, z, y, c, :, lanes(x, 256)], lsem.at[2]),
        pltpu.make_async_copy(gain_hbm, gains.at[x], lsem.at[3]),
        pltpu.make_async_copy(tok_hbm.at[pl.ds(x * 192, 192), :], btok.at[:, lanes(x, F)], lsem.at[4]),
    ]
    for load in loads:
        load.start()
    w_hbm = (wg_hbm, wu_hbm, wd_hbm)
    w_loads = [pltpu.make_async_copy(w_hbm[k], weights.at[k, x], lsem.at[5 + k]) for k in range(3)]

    @pl.when(primary)
    def _():
        for load in w_loads:
            load.start()

    experts = lax.broadcasted_iota(jnp.int32, (64, T), 0)
    r0, r1 = rout_t[0:1, :], rout_t[1:2, :]
    named0, named1 = experts == r0, experts == r1
    one_hot = jnp.where(named0 | named1, 1.0, 0.0).astype(jnp.bfloat16)
    earlier = jnp.where(
        lax.broadcasted_iota(jnp.int32, (T, T), 0) < lax.broadcasted_iota(jnp.int32, (T, T), 1), 1.0, 0.0
    ).astype(jnp.bfloat16)
    before = jnp.dot(one_hot, earlier, preferred_element_type=jnp.float32)
    slot0 = r0 * CAP + jnp.sum(jnp.where(named0, before, 0.0), axis=0, keepdims=True).astype(jnp.int32)
    slot1 = r1 * CAP + jnp.sum(jnp.where(named1, before, 0.0), axis=0, keepdims=True).astype(jnp.int32)
    slots_v[0:1, :] = slot0.astype(jnp.float32)
    slots_v[1:2, :] = slot1.astype(jnp.float32)
    slots_v[2:4, :] = rw_t[...]
    slots_v[4:8, :] = jnp.zeros((4, T), jnp.float32)

    for load in loads:
        load.wait()

    def dispatch_copy(q, j):
        m = block_at(q)
        r, e, xx = target_of(m, j)
        return remote(
            send.at[m, pl.ds(pl.multiple_of(r * CAP, 16), CAP), :],
            land.at[m_own, :, lanes(x, F)],
            esend.at[q * 4 + j],
            erecv.at[m_own * 4 + x],
            e,
            xx,
        )

    def pack(q, carry):
        m = block_at(q)
        slots = lax.broadcasted_iota(jnp.int32, (BLK, T), 0) + m * BLK
        pick = jnp.where((slots == slot0) | (slots == slot1), 1.0, 0.0).astype(jnp.bfloat16)
        send[m] = jnp.dot(pick, tok[...], preferred_element_type=jnp.float32).astype(jnp.bfloat16)
        return carry

    def dispatch(q, carry):
        for j in range(4):
            if j == 0:
                own = (q == 0) & is_self

                @pl.when(jnp.logical_not(own))
                def _():
                    dispatch_copy(q, j).start()

                @pl.when(own)
                def _():
                    r, _, _ = target_of(m_own, 0)
                    land[m_own, :, lanes(x, F)] = send[m_own, pl.ds(pl.multiple_of(r * CAP, 16), CAP), :]
            else:
                dispatch_copy(q, j).start()
        return carry

    def pack_and_send(q, carry):
        return dispatch(q, pack(q, carry))

    lax.fori_loop(0, EARLY, pack, 0)
    pl.semaphore_wait(barrier, 13 + 128 - 2 * is_self.astype(jnp.int32))

    mate = (x + 5 - 2 * rel) % 4
    outer = (x + 3 + 2 * rel) % 4
    inner = (x + 2 * rel + 3) % 4

    def w_own(k, to):
        return remote(w_hbm[k], weights.at[k, x], wsend.at[k], wrecv.at[k, x], ep, to)

    def w_piece(k, slot, sem, e, to):
        return remote(weights.at[k, slot], weights.at[k, slot], sem, wrecv.at[k, slot], e, to)

    def w_forward(k):
        return w_piece(k, outer, fsend.at[k], ep, mate)

    def w_across(k, slot):
        return w_piece(k, slot, csend.at[k, slot], ep_of(z, y, 1 - c), x)

    def w_start(ks):
        @pl.when(primary)
        def _():
            for k in ks:
                w_own(k, mate).start()

        @pl.when(jnp.logical_not(primary))
        def _():
            for k in ks:
                w_own(k, inner).start()

    def z_copy(d):
        zz = (z + d) % 8
        mine = bw.at[:, z, y, c, :, lanes(x, 256)]
        return remote(mine, mine, zsend.at[d], zrecv.at[d], ep_of(zz, y, c), x)

    def x_copy(k, d):
        mine = bw.at[k, :, y, c, :, lanes(x, 256)]
        return remote(mine, mine, xsend.at[k, d], xrecv.at[k, d], ep, (x + d) % 4)

    def y_copy(k, way):
        mine = bw.at[k, :, y, c]
        return remote(mine, mine, ysend.at[k, way], yrecv.at[k, way], ep_of(z, (y + (1, 3)[way]) % 4, c), x)

    def y_forward(way):
        slot = (y + (3, 1)[way]) % 4
        piece = bw.at[way, :, slot, c]
        return remote(piece, piece, ysend.at[2, way], yrecv.at[2, way], ep_of(z, (y + (1, 3)[way]) % 4, c), x)

    def d_copy(k):
        mine = bw.at[k, :, :, c]
        return remote(mine, mine, dsend.at[k], drecv.at[k], ep_of(z, y, 1 - c), x)

    def gain_copy(d):
        return remote(gains.at[x], gains.at[x], gsend.at[d], grecv.at[d], ep, (x + d) % 4)

    def btok_copy(d):
        xx = (x + d) % 4
        return remote(
            tok.at[pl.ds(xx * 192, 192), :], btok.at[:, lanes(x, F)], btsend.at[d], btrecv.at[d], ep, xx
        )

    for d in range(1, 8):
        z_copy(d).start()
    for d in range(1, 4):
        gain_copy(d).start()
    w_start((0, 1, 2))
    lax.fori_loop(0, FIRST, dispatch, 0)

    @pl.when(primary)
    def _():
        for k in range(3):
            w_loads[k].wait()
            w_across(k, x).start()

    for d in range(1, 8):
        z_copy(d).wait_recv()
    for d in range(1, 4):
        for k in range(2):
            x_copy(k, d).start()
    lax.fori_loop(FIRST, EARLY, dispatch, 0)
    lax.fori_loop(EARLY, NQ, pack_and_send, 0)

    @pl.when(primary)
    def _():
        for k in range(3):
            w_piece(k, outer, fsend.at[k], ep, x).wait_recv()
            w_forward(k).start()
            w_across(k, outer).start()
            w_piece(k, mate, fsend.at[k], ep, x).wait_recv()
            w_across(k, mate).start()

    for d in range(1, 4):
        for k in range(2):
            x_copy(k, d).wait_recv()
    for way in range(2):
        for k in range(2):
            y_copy(k, way).start()
    for d in range(1, 4):
        btok_copy(d).start()

    @pl.when(primary)
    def _():
        for k in range(3):
            w_piece(k, (x + 2) % 4, fsend.at[k], ep, x).wait_recv()
            w_across(k, (x + 2) % 4).start()

    for d in range(1, 4):
        gain_copy(d).wait_recv()

    @pl.when(jnp.logical_not(primary))
    def _():
        for k in range(3):
            for h in range(4):
                w_piece(k, h, fsend.at[k], ep, x).wait_recv()

    for way in range(2):
        for k in range(2):
            y_copy(k, way).wait_recv()
    for way in range(2):
        y_forward(way).start()

    def norm_rows(source, target):
        floats = source.astype(jnp.float32)
        squares = jnp.sum(floats * floats, axis=1, keepdims=True)
        scaled = floats * lax.rsqrt(squares * (1.0 / (4 * F)) + EPSILON)
        for k in range(4):
            target[:, k * F : (k + 1) * F] = (scaled[:, k * F : (k + 1) * F] * gains[k]).astype(jnp.bfloat16)

    def arrival(m, xx):
        there = land.at[m, :, lanes(xx, F)]
        return remote(there, there, esend.at[0], erecv.at[m * 4 + xx], ep, xx)

    def return_copy(jj, m):
        quarter = (x + (0, 1, 3, 2)[jj]) % 4
        return remote(
            result.at[quarter, m], ret.at[served], rsend.at[jj * 16 + m], rrecv.at[served], m * 4 + sigma, quarter
        )

    def expert(i, carry):
        part = (z // 2 + i) % 4
        for mm in range(4):
            m = part * 4 + mm
            for xx in range(4):

                @pl.when(jnp.logical_not(is_self & (m == m_own) & (x == xx)))
                def _():
                    arrival(m, xx).wait_recv()

        def one(r, inner):
            m, row = part * 4 + r // 3, pl.multiple_of((r % 3) * 16, 16)
            norm_rows(land[m, pl.ds(row, 16), :], normed.at[pl.ds(pl.multiple_of(r * 16, 16), 16), :])
            return inner

        lax.fori_loop(0, 12, one, 0)
        for n in range(2):
            cols = slice(n * 256, n * 256 + 256)
            sums = []
            for k in range(2):
                total = jnp.dot(normed[:, 0:F], weights[k, 0, :, cols], preferred_element_type=jnp.float32)
                for h in range(1, 4):
                    total += jnp.dot(
                        normed[:, h * F : (h + 1) * F], weights[k, h, :, cols], preferred_element_type=jnp.float32
                    )
                sums.append(total)
            gate_sum, up_sum = sums
            hidden[:, cols] = (gate_sum / (1.0 + jnp.exp(-gate_sum)) * up_sum).astype(jnp.bfloat16)
        for jj in range(4):
            quarter = (x + (0, 1, 3, 2)[jj]) % 4
            rows = jnp.dot(hidden[...], weights[2, quarter], preferred_element_type=jnp.float32)
            result[quarter, pl.ds(part * 4, 4)] = rows.astype(jnp.bfloat16).reshape(4, CAP, F)
            for mm in range(4):
                m = part * 4 + mm
                if jj == 0:
                    own = is_self & (m == m_own)

                    @pl.when(jnp.logical_not(own))
                    def _():
                        return_copy(jj, m).start()

                    @pl.when(own)
                    def _():
                        ret[served] = result[x, m_own]
                else:
                    return_copy(jj, m).start()

        @pl.when(i == 2)
        def _():
            for way in range(2):
                y_forward(way).wait_recv()
            for k in range(2):
                d_copy(k).start()

        return carry

    lax.fori_loop(0, 4, expert, 0)

    for d in range(1, 4):
        btok_copy(d).wait_recv()

    def branch_norm(r, carry):
        rows = pl.ds(pl.multiple_of(r * 16, 16), 16)
        norm_rows(btok[rows, :], bnorm.at[rows, :])
        return carry

    lax.fori_loop(0, 12, branch_norm, 0)

    columns = slots_v[...].T
    place0, place1, rw0, rw1 = (columns[:, k : k + 1] for k in range(4))

    for k in range(2):
        d_copy(k).wait_recv()

    w_in = bw.at[0].reshape(2048, 1024)
    w_out = bw.at[1].reshape(2048, 1024)
    for n in range(4):
        cols = slice(n * 256, n * 256 + 256)
        total = jnp.dot(bnorm[...], w_in[:, cols], preferred_element_type=jnp.float32)
        bhid[:, cols] = (total / (1.0 + jnp.exp(-total))).astype(jnp.bfloat16)

    def bret_copy(d):
        xx = (x + d) % 4
        return remote(
            bres.at[xx], bret.at[pl.ds(x * 192, 192), :], brsend.at[d], brrecv.at[d], ep, xx
        )

    for d in (1, 3, 2, 0):
        quarter = (x + d) % 4
        rows = lax.dot_general(
            bhid[...],
            w_out[pl.ds(pl.multiple_of(quarter * F, F), F), :],
            (((1,), (1,)), ((), ())),
            preferred_element_type=jnp.float32,
        )
        if d == 0:
            bret[pl.ds(pl.multiple_of(x * 192, 192), 192), :] = rows.astype(jnp.bfloat16)
        else:
            bres[quarter] = rows.astype(jnp.bfloat16)
            bret_copy(d).start()

    for d in range(1, 8):
        z_copy(d).wait_send()
    for d in range(1, 4):
        gain_copy(d).wait_send()
        btok_copy(d).wait_send()
        for k in range(2):
            x_copy(k, d).wait_send()
    for way in range(2):
        for k in range(2):
            y_copy(k, way).wait_send()
        y_forward(way).wait_send()
    for k in range(2):
        d_copy(k).wait_send()
    for k in range(3):
        w_own(k, x).wait_send()

    @pl.when(primary)
    def _():
        for k in range(3):
            w_forward(k).wait_send()
            for h in range(4):
                w_across(k, h).wait_send()

    def dispatched(q, carry):
        for j in range(4):
            if j == 0:

                @pl.when(jnp.logical_not((q == 0) & is_self))
                def _():
                    dispatch_copy(q, j).wait_send()
            else:
                dispatch_copy(q, j).wait_send()
        return carry

    lax.fori_loop(0, NQ, dispatched, 0)

    acc[...] = jnp.zeros_like(acc)

    def returned(e):
        return remote(ret.at[e], ret.at[e], rsend.at[0], rrecv.at[e], ep, x)

    def combine(i, carry):
        part = (z // 2 + i) % 4

        def wait(k, inner):
            e = part * 16 + k

            @pl.when(jnp.logical_not(is_self & (e == served)))
            def _():
                returned(e).wait_recv()

            return inner

        lax.fori_loop(0, 16, wait, 0)
        rows = ret[pl.ds(part * 16, 16)].reshape(16 * CAP, F)
        for h in range(3):
            sl = slice(h * 256, h * 256 + 256)
            slots = (lax.broadcasted_iota(jnp.int32, (256, 16 * CAP), 1) + part * (16 * CAP)).astype(jnp.float32)
            mix = jnp.where(slots == place0[sl], rw0[sl], 0.0) + jnp.where(slots == place1[sl], rw1[sl], 0.0)
            acc[sl, :] += jnp.dot(mix.astype(jnp.bfloat16), rows, preferred_element_type=jnp.float32)
        return carry

    lax.fori_loop(0, 4, combine, 0)
    for d in range(1, 4):
        bret_copy(d).wait_recv()
    share = 1.0 / (1.0 + jnp.exp(-gate_ref[0:1, :]))
    for h in range(3):
        sl = slice(h * 256, h * 256 + 256)
        out_ref[sl, :] = (acc[sl, :] + share * bret[sl, :].astype(jnp.float32)).astype(jnp.bfloat16)

    for d in range(1, 4):
        bret_copy(d).wait_send()

    def sent(q, carry):
        for j in range(4):
            if j == 0:

                @pl.when(jnp.logical_not((q == m_own) & is_self))
                def _():
                    return_copy(j, q).wait_send()
            else:
                return_copy(j, q).wait_send()
        return carry

    lax.fori_loop(0, NQ, sent, 0)


def body(
    tokens, norm_gain, routing, route_weight, w_gate, w_up, w_down, w_branch_in, w_branch_out, branch_gate
):
    bf16, f32 = jnp.bfloat16, jnp.float32
    vmem = pl.BlockSpec(memory_space=pltpu.VMEM)
    hbm = pl.BlockSpec(memory_space=pl.ANY)
    dma = pltpu.SemaphoreType.DMA
    return pl.pallas_call(
        kernel,
        out_shape=jax.ShapeDtypeStruct((T, F), bf16),
        in_specs=[hbm, hbm, vmem, vmem, hbm, hbm, hbm, hbm, hbm, vmem],
        out_specs=vmem,
        scratch_shapes=[
            pltpu.VMEM((T, F), bf16),
            pltpu.VMEM((4, 1, F), f32),
            pltpu.VMEM((NQ, BLK, F), bf16),
            pltpu.VMEM((NQ, CAP, 4 * F), bf16),
            pltpu.VMEM((3, 4, 512, 512), bf16),
            pltpu.VMEM((2, 8, 4, 2, 32, 1024), bf16),
            pltpu.VMEM((BLK, 4 * F), bf16),
            pltpu.VMEM((BLK, 512), bf16),
            pltpu.VMEM((4, NQ, CAP, F), bf16),
            pltpu.VMEM((64, CAP, F), bf16),
            pltpu.VMEM((192, 4 * F), bf16),
            pltpu.VMEM((192, 4 * F), bf16),
            pltpu.VMEM((192, 1024), bf16),
            pltpu.VMEM((4, 192, F), bf16),
            pltpu.VMEM((T, F), bf16),
            pltpu.VMEM((T, F), f32),
            pltpu.VMEM((8, T), f32),
            dma((8,)),
            dma((4,)), dma((4,)),
            dma((4,)), dma((4,)),
            dma((4,)), dma((4,)),
            dma((8,)), dma((8,)),
            dma((2, 4)), dma((2, 4)),
            dma((3, 2)), dma((3, 2)),
            dma((2,)), dma((2,)),
            dma((3,)), dma((3, 4)),
            dma((3,)), dma((3, 4)),
            dma((64,)), dma((64,)),
            dma((64,)), dma((64,)),
        ],
        compiler_params=pltpu.CompilerParams(collective_id=0, has_side_effects=True, vmem_limit_bytes=60 * 1024 * 1024),
        name="layer",
    )(
        tokens,
        norm_gain.reshape(1, F),
        routing.T,
        route_weight.T,
        w_gate[0],
        w_up[0],
        w_down[0],
        w_branch_in,
        w_branch_out.T,
        branch_gate.reshape(1, F),
    )


def solution(mesh):
    return jax.shard_map(
        body,
        mesh=mesh,
        in_specs=(
            P("ep", "tp"),
            P("tp"),
            P("ep", None),
            P("ep", None),
            P("ep", "tp", None),
            P("ep", "tp", None),
            P("ep", None, "tp"),
            P("ep", "tp"),
            P("tp", "ep"),
            P("tp"),
        ),
        out_specs=P("ep", "tp"),
        check_vma=False,
    )
```

time: 224 us -> 194 us (0.87); the launches traced: 222 us -> 190 us
  Pallas kernels: 216 us -> 188 us
  local copies, waits for them, and re-layouts: 5.92 us -> 2.06 us
    pallas_call x1, Pallas kernels: 216 us -> 188 us  [body(): pl.pallas_call(kernel, out_shape=jax.ShapeDtypeStruct((T, F), bf16), in_s...]
    unnamed x15 -> x1, local copies, waits for them, and re-layouts: 4.72 us -> 2.06 us
where the time goes in v2:
time: 194 us; the launch traced here: 190 us
  Pallas kernels  188 us (97%)
  local copies, waits for them, and re-layouts  2.06 us (1%)
    pallas_call x1, Pallas kernels, body(): pl.pallas_call(kernel, out_shape=jax.ShapeDtypeStruct((T, F), bf16), in_s...  188 us

profile of v2, /device:TPU:32, one launch (start us, length us, event | category | flops | bytes accessed | tf_op | source)
XLA Modules:
  0.0 189.9 jit_solution(13384476980694002894)
XLA Ops:
  0.0 187.8 %layer.1 = bf16[768,512]{1,0:T(8,128)(2,1)} custom-call(bf16[768,512]{1,0:T(8,128)(2,1)} %tok_hbm.1, f32[1,512]{1,0:T(1,128)} %bitcast.14, s32[2,768]{1,0:T(2,128)} %bitcast.12, f32[2,768]{1,0:T(2,128)} %bitcast.13, bf16[512,512]{1,0:T(8,128)(2,1)} %bitcast.8, bf16[512,512]{1,0:T(8,128)(2,1)} %bitcast.9, bf16[512,512]{1,0:T(8,128)(2,1)} %bitcast.10, ...), custom_call_target="tpu_custom_call" | custom-call | tf_op jit(solution)/shard_map/layer/pallas_call | solution.py:495
  187.8 2.1 %copy.12 = bf16[768,512]{1,0:T(8,128)(2,1)} copy(bf16[768,512]{1,0:T(8,128)(2,1)} %layer.1) | data formatting | bytes 1572864

commit v3 on v2

--- a/solution.py
+++ b/solution.py
@@ -1,5 +1,3 @@
-import functools
-
 import jax
 import jax.numpy as jnp
 from jax import lax
@@ -14,16 +12,18 @@
 T = 768
 NQ = 16
 BLK = 4 * CAP
-EARLY = 14
-FIRST = 4
+GT = 384
+MEM = 16
+FIRST, SECOND = 3, 6
 
 
 def kernel(
     tok_hbm, gain_hbm, rout_t, rw_t, wg_hbm, wu_hbm, wd_hbm, bwi_hbm, bwo_hbm, gate_ref,
     out_ref,
-    tok, gains, send, land, weights, bw, normed, hidden, result, ret, btok, bnorm, bhid, bres, bret, acc, slots_v,
+    tok, gains, send, land, weights, bw, normed, hidden, result, rr, btok, bnorm, bhid, bres, bret, acc, gslot_v,
+    meta_out, meta, mix, rq, back,
     lsem, gsend, grecv, btsend, btrecv, brsend, brrecv, zsend, zrecv, xsend, xrecv, ysend, yrecv, dsend, drecv,
-    wsend, wrecv, fsend, csend, esend, erecv, rsend, rrecv,
+    wsend, wrecv, fsend, csend, esend, erecv, rsend, rrecv, msend, mrecv, s4send, s4recv,
 ):
     ep = lax.axis_index("ep")
     x = lax.axis_index("tp")
@@ -57,6 +57,15 @@
         r = (h - s4 + 4) % 4
         return r, m * 4 + 2 * (r // 2) + h % 2, xx
 
+    group, mine_in = z // 2, served % MEM
+
+    def relay_of(zz, g):
+        ahead = (2 * g - zz + 16) % 8
+        return jnp.where(ahead <= 3, 2 * g, 2 * g + 1), jnp.where(ahead <= 3, ahead, 7 - ahead)
+
+    def source_z(k):
+        return jnp.where(z % 2 == 0, z - k + 8, z + k) % 8
+
     barrier = pltpu.get_barrier_semaphore()
 
     def greet_one(e, xx):
@@ -66,21 +75,24 @@
         greet_one(ep_of((z + d) % 8, y, c), x)
     for d in range(1, 4):
         greet_one(ep, (x + d) % 4)
+        greet_one(ep_of(source_z(d), y, c), x)
+        greet_one(ep_of(relay_of(z, (group + d) % 4)[0], y, c), x)
     for d in (1, 3):
         greet_one(ep_of(z, (y + d) % 4, c), x)
     greet_one(ep_of(z, y, 1 - c), x)
 
     def greet(m, carry):
         for j in range(4):
-            _, e, xx = target_of(m, j)
-
-            @pl.when(jnp.logical_not((e == ep) & (xx == x)))
-            def _():
-                greet_one(e, xx)
 
             @pl.when(jnp.logical_not(is_self & (m == m_own) & (j == 0)))
             def _():
-                greet_one(m * 4 + sigma, xx)
+                greet_one(m * 4 + sigma, (x + j) % 4)
+
+        @pl.when(jnp.logical_not(is_self & (m == mine_in)))
+        def _():
+            h = (s4 + m) % 4
+            greet_one(group * MEM + (m // 2) * 2 + h % 2, 2 * (m % 2) + h // 2)
+
         return carry
 
     lax.fori_loop(0, NQ, greet, 0)
@@ -105,17 +117,37 @@
     experts = lax.broadcasted_iota(jnp.int32, (64, T), 0)
     r0, r1 = rout_t[0:1, :], rout_t[1:2, :]
     named0, named1 = experts == r0, experts == r1
-    one_hot = jnp.where(named0 | named1, 1.0, 0.0).astype(jnp.bfloat16)
+    gid = r0 // MEM
+    in_group = lax.broadcasted_iota(jnp.int32, (16, T), 0) == gid
+    one_hot = jnp.concatenate(
+        [
+            jnp.where(named0 | named1, 1.0, 0.0).astype(jnp.bfloat16),
+            jnp.where(in_group, 1.0, 0.0).astype(jnp.bfloat16),
+        ],
+        axis=0,
+    )
     earlier = jnp.where(
         lax.broadcasted_iota(jnp.int32, (T, T), 0) < lax.broadcasted_iota(jnp.int32, (T, T), 1), 1.0, 0.0
     ).astype(jnp.bfloat16)
     before = jnp.dot(one_hot, earlier, preferred_element_type=jnp.float32)
-    slot0 = r0 * CAP + jnp.sum(jnp.where(named0, before, 0.0), axis=0, keepdims=True).astype(jnp.int32)
-    slot1 = r1 * CAP + jnp.sum(jnp.where(named1, before, 0.0), axis=0, keepdims=True).astype(jnp.int32)
-    slots_v[0:1, :] = slot0.astype(jnp.float32)
-    slots_v[1:2, :] = slot1.astype(jnp.float32)
-    slots_v[2:4, :] = rw_t[...]
-    slots_v[4:8, :] = jnp.zeros((4, T), jnp.float32)
+    pos0 = jnp.sum(jnp.where(named0, before[:64], 0.0), axis=0, keepdims=True)
+    pos1 = jnp.sum(jnp.where(named1, before[:64], 0.0), axis=0, keepdims=True)
+    rank = jnp.sum(jnp.where(in_group, before[64:], 0.0), axis=0, keepdims=True)
+    slot0 = r0 * CAP + pos0.astype(jnp.int32)
+    slot1 = r1 * CAP + pos1.astype(jnp.int32)
+    gslot = (gid * GT).astype(jnp.float32) + rank
+    gslot_v[...] = jnp.broadcast_to(gslot, (8, T))
+    facts = jnp.concatenate(
+        [
+            (r0 - gid * MEM).astype(jnp.float32),
+            pos0,
+            (r1 - gid * MEM).astype(jnp.float32),
+            pos1,
+            rw_t[...],
+            jnp.zeros((2, T), jnp.float32),
+        ],
+        axis=0,
+    ).astype(jnp.bfloat16)
 
     for load in loads:
         load.wait()
@@ -139,28 +171,27 @@
         send[m] = jnp.dot(pick, tok[...], preferred_element_type=jnp.float32).astype(jnp.bfloat16)
         return carry
 
-    def dispatch(q, carry):
-        for j in range(4):
-            if j == 0:
-                own = (q == 0) & is_self
-
-                @pl.when(jnp.logical_not(own))
-                def _():
-                    dispatch_copy(q, j).start()
-
-                @pl.when(own)
-                def _():
-                    r, _, _ = target_of(m_own, 0)
-                    land[m_own, :, lanes(x, F)] = send[m_own, pl.ds(pl.multiple_of(r * CAP, 16), CAP), :]
-            else:
-                dispatch_copy(q, j).start()
-        return carry
-
-    def pack_and_send(q, carry):
-        return dispatch(q, pack(q, carry))
-
-    lax.fori_loop(0, EARLY, pack, 0)
-    pl.semaphore_wait(barrier, 13 + 128 - 2 * is_self.astype(jnp.int32))
+    def dispatch_straight(q, carry):
+        own = (q == 0) & is_self
+
+        @pl.when(jnp.logical_not(own))
+        def _():
+            dispatch_copy(q, 0).start()
+
+        @pl.when(own)
+        def _():
+            r, _, _ = target_of(m_own, 0)
+            land[m_own, :, lanes(x, F)] = send[m_own, pl.ds(pl.multiple_of(r * CAP, 16), CAP), :]
+
+        return carry
+
+    def dispatch_across(q, carry):
+        for j in range(1, 4):
+            dispatch_copy(q, j).start()
+        return carry
+
+    lax.fori_loop(0, NQ, pack, 0)
+    pl.semaphore_wait(barrier, 13 + 6 + 64 + 16 - 2 * is_self.astype(jnp.int32))
 
     mate = (x + 5 - 2 * rel) % 4
     outer = (x + 3 + 2 * rel) % 4
@@ -224,8 +255,8 @@
         z_copy(d).start()
     for d in range(1, 4):
         gain_copy(d).start()
-    w_start((0, 1, 2))
-    lax.fori_loop(0, FIRST, dispatch, 0)
+    w_start((0, 1))
+    lax.fori_loop(0, NQ, dispatch_straight, 0)
 
     @pl.when(primary)
     def _():
@@ -233,52 +264,97 @@
             w_loads[k].wait()
             w_across(k, x).start()
 
+    def w_relay(k):
+        w_piece(k, outer, fsend.at[k], ep, x).wait_recv()
+        w_forward(k).start()
+        w_across(k, outer).start()
+        w_piece(k, mate, fsend.at[k], ep, x).wait_recv()
+        w_across(k, mate).start()
+
+    def w_last(k):
+        w_piece(k, (x + 2) % 4, fsend.at[k], ep, x).wait_recv()
+        w_across(k, (x + 2) % 4).start()
+
+    def w_served(k):
+        for h in range(4):
+            w_piece(k, h, fsend.at[k], ep, x).wait_recv()
+
     for d in range(1, 8):
         z_copy(d).wait_recv()
     for d in range(1, 4):
         for k in range(2):
             x_copy(k, d).start()
-    lax.fori_loop(FIRST, EARLY, dispatch, 0)
-    lax.fori_loop(EARLY, NQ, pack_and_send, 0)
+
+    lax.fori_loop(0, FIRST, dispatch_across, 0)
+
+    def m_copy(d):
+        g = (group + d) % 4
+        plane, k = relay_of(z, g)
+        return remote(meta_out.at[g], meta.at[k], msend.at[d], mrecv.at[k], ep_of(plane, y, c), x)
+
+    for d in range(4):
+        g = (group + d) % 4
+        places = (lax.broadcasted_iota(jnp.int32, (GT, T), 0) + g * GT).astype(jnp.float32)
+        pick = jnp.where(places == gslot, 1.0, 0.0).astype(jnp.bfloat16)
+        told = lax.dot_general(facts, pick, (((1,), (1,)), ((), ())), preferred_element_type=jnp.float32)
+        if d == 0:
+            meta[0] = told
+        else:
+            meta_out[g] = told
+            m_copy(d).start()
+
 
     @pl.when(primary)
     def _():
-        for k in range(3):
-            w_piece(k, outer, fsend.at[k], ep, x).wait_recv()
-            w_forward(k).start()
-            w_across(k, outer).start()
-            w_piece(k, mate, fsend.at[k], ep, x).wait_recv()
-            w_across(k, mate).start()
-
+        for k in range(2):
+            w_relay(k)
+
+    lax.fori_loop(FIRST, SECOND, dispatch_across, 0)
     for d in range(1, 4):
         for k in range(2):
             x_copy(k, d).wait_recv()
     for way in range(2):
         for k in range(2):
             y_copy(k, way).start()
-    for d in range(1, 4):
-        btok_copy(d).start()
+    lax.fori_loop(SECOND, NQ, dispatch_across, 0)
+    w_start((2,))
+
+    for k in range(1, 4):
+        remote(meta.at[k], meta.at[k], msend.at[0], mrecv.at[k], ep, x).wait_recv()
+    for k in range(4):
+        columns = meta[k].T
+        at0 = columns[:, 0:1] * CAP + columns[:, 1:2]
+        at1 = columns[:, 2:3] * CAP + columns[:, 3:4]
+        for h in range(2):
+            sl = slice(h * 192, h * 192 + 192)
+            slots = lax.broadcasted_iota(jnp.int32, (192, T), 1).astype(jnp.float32)
+            mix[k, sl, :] = (
+                jnp.where(slots == at0[sl], columns[sl, 4:5], 0.0)
+                + jnp.where(slots == at1[sl], columns[sl, 5:6], 0.0)
+            ).astype(jnp.bfloat16)
 
     @pl.when(primary)
     def _():
-        for k in range(3):
-            w_piece(k, (x + 2) % 4, fsend.at[k], ep, x).wait_recv()
-            w_across(k, (x + 2) % 4).start()
-
-    for d in range(1, 4):
-        gain_copy(d).wait_recv()
-
-    @pl.when(jnp.logical_not(primary))
-    def _():
-        for k in range(3):
-            for h in range(4):
-                w_piece(k, h, fsend.at[k], ep, x).wait_recv()
+        w_relay(2)
 
     for way in range(2):
         for k in range(2):
             y_copy(k, way).wait_recv()
     for way in range(2):
         y_forward(way).start()
+
+    @pl.when(primary)
+    def _():
+        for k in range(2):
+            w_last(k)
+
+    for d in range(1, 4):
+        gain_copy(d).wait_recv()
+
+    @pl.when(jnp.logical_not(primary))
+    def _():
+        for k in range(2):
+            w_served(k)
 
     def norm_rows(source, target):
         floats = source.astype(jnp.float32)
@@ -293,12 +369,36 @@
 
     def return_copy(jj, m):
         quarter = (x + (0, 1, 3, 2)[jj]) % 4
+        plane, k = relay_of(m // 2, group)
         return remote(
-            result.at[quarter, m], ret.at[served], rsend.at[jj * 16 + m], rrecv.at[served], m * 4 + sigma, quarter
+            result.at[quarter, m], rr.at[k, mine_in], rsend.at[jj * 16 + m], rrecv.at[k * MEM + mine_in],
+            ep_of(plane, (m % 2) * 2 + sigma // 2, sigma % 2), quarter,
         )
 
+    def stays(m):
+        return is_self & (m % 2 == y // 2) & (relay_of(m // 2, group)[0] == z)
+
+    def pair_at(i):
+        return jnp.where(i == 0, 2, jnp.where(i == 1, 1, jnp.where(i == 2, 3, 0)))
+
+    def give_back(part, jj):
+        for mm in range(4):
+            m = part * 4 + mm
+            if jj == 0:
+                own = stays(m)
+
+                @pl.when(jnp.logical_not(own))
+                def _():
+                    return_copy(jj, m).start()
+
+                @pl.when(own)
+                def _():
+                    rr[relay_of(m // 2, group)[1], mine_in] = result[x, m]
+            else:
+                return_copy(jj, m).start()
+
     def expert(i, carry):
-        part = (z // 2 + i) % 4
+        part = (z // 2 + pair_at(i)) % 4
         for mm in range(4):
             m = part * 4 + mm
             for xx in range(4):
@@ -325,36 +425,58 @@
                 sums.append(total)
             gate_sum, up_sum = sums
             hidden[:, cols] = (gate_sum / (1.0 + jnp.exp(-gate_sum)) * up_sum).astype(jnp.bfloat16)
+
+        @pl.when((i == 0) & primary)
+        def _():
+            w_last(2)
+
+        @pl.when((i == 0) & jnp.logical_not(primary))
+        def _():
+            w_served(2)
+
         for jj in range(4):
             quarter = (x + (0, 1, 3, 2)[jj]) % 4
             rows = jnp.dot(hidden[...], weights[2, quarter], preferred_element_type=jnp.float32)
             result[quarter, pl.ds(part * 4, 4)] = rows.astype(jnp.bfloat16).reshape(4, CAP, F)
-            for mm in range(4):
-                m = part * 4 + mm
-                if jj == 0:
-                    own = is_self & (m == m_own)
-
-                    @pl.when(jnp.logical_not(own))
-                    def _():
-                        return_copy(jj, m).start()
-
-                    @pl.when(own)
-                    def _():
-                        ret[served] = result[x, m_own]
-                else:
-                    return_copy(jj, m).start()
-
-        @pl.when(i == 2)
-        def _():
-            for way in range(2):
-                y_forward(way).wait_recv()
-            for k in range(2):
-                d_copy(k).start()
+
+            @pl.when(i < 3)
+            def _():
+                give_back(part, jj)
 
         return carry
 
     lax.fori_loop(0, 4, expert, 0)
-
+    for d in range(1, 4):
+        btok_copy(d).start()
+
+    def s4_copy(k):
+        return remote(rq.at[k], back.at[group], s4send.at[k], s4recv.at[group], ep_of(source_z(k), y, c), x)
+
+    def relay(k):
+        def wait(n, inner):
+            @pl.when(jnp.logical_not(is_self & (n == mine_in)))
+            def _():
+                remote(rr.at[k, n], rr.at[k, n], rsend.at[0], rrecv.at[k * MEM + n], ep, x).wait_recv()
+
+            return inner
+
+        lax.fori_loop(0, MEM, wait, 0)
+        total = jnp.dot(mix[k], rr[k].reshape(T, F), preferred_element_type=jnp.float32).astype(jnp.bfloat16)
+        if k == 0:
+            back[group] = total
+        else:
+            rq[k] = total
+            s4_copy(k).start()
+
+    for way in range(2):
+        y_forward(way).wait_recv()
+    for k in range(2):
+        d_copy(k).start()
+    relay(3)
+    for jj in range(4):
+        give_back(group, jj)
+    relay(2)
+    relay(1)
     for d in range(1, 4):
         btok_copy(d).wait_recv()
 
@@ -364,9 +486,6 @@
         return carry
 
     lax.fori_loop(0, 12, branch_norm, 0)
-
-    columns = slots_v[...].T
-    place0, place1, rw0, rw1 = (columns[:, k : k + 1] for k in range(4))
 
     for k in range(2):
         d_copy(k).wait_recv()
@@ -434,48 +553,38 @@
 
     lax.fori_loop(0, NQ, dispatched, 0)
 
-    acc[...] = jnp.zeros_like(acc)
-
-    def returned(e):
-        return remote(ret.at[e], ret.at[e], rsend.at[0], rrecv.at[e], ep, x)
-
-    def combine(i, carry):
-        part = (z // 2 + i) % 4
-
-        def wait(k, inner):
-            e = part * 16 + k
-
-            @pl.when(jnp.logical_not(is_self & (e == served)))
-            def _():
-                returned(e).wait_recv()
-
-            return inner
-
-        lax.fori_loop(0, 16, wait, 0)
-        rows = ret[pl.ds(part * 16, 16)].reshape(16 * CAP, F)
+    relay(0)
+
+    place = gslot_v[...].T[:, 0:1]
+    for d in range(1, 4):
+        bret_copy(d).wait_recv()
+    share = 1.0 / (1.0 + jnp.exp(-gate_ref[0:1, :]))
+    for n, d in enumerate((0, 1, 3, 2)):
+        g = (group + d) % 4
+        if d > 0:
+            remote(back.at[g], back.at[g], s4send.at[0], s4recv.at[g], ep, x).wait_recv()
         for h in range(3):
             sl = slice(h * 256, h * 256 + 256)
-            slots = (lax.broadcasted_iota(jnp.int32, (256, 16 * CAP), 1) + part * (16 * CAP)).astype(jnp.float32)
-            mix = jnp.where(slots == place0[sl], rw0[sl], 0.0) + jnp.where(slots == place1[sl], rw1[sl], 0.0)
-            acc[sl, :] += jnp.dot(mix.astype(jnp.bfloat16), rows, preferred_element_type=jnp.float32)
-        return carry
-
-    lax.fori_loop(0, 4, combine, 0)
-    for d in range(1, 4):
-        bret_copy(d).wait_recv()
-    share = 1.0 / (1.0 + jnp.exp(-gate_ref[0:1, :]))
-    for h in range(3):
-        sl = slice(h * 256, h * 256 + 256)
-        out_ref[sl, :] = (acc[sl, :] + share * bret[sl, :].astype(jnp.float32)).astype(jnp.bfloat16)
+            places = (lax.broadcasted_iota(jnp.int32, (256, GT), 1) + g * GT).astype(jnp.float32)
+            pick = jnp.where(places == place[sl], 1.0, 0.0).astype(jnp.bfloat16)
+            total = jnp.dot(pick, back[g], preferred_element_type=jnp.float32)
+            if n == 0:
+                acc[sl, :] = total + share * bret[sl, :].astype(jnp.float32)
+            elif n < 3:
+                acc[sl, :] += total
+            else:
+                out_ref[sl, :] = (acc[sl, :] + total).astype(jnp.bfloat16)
 
     for d in range(1, 4):
         bret_copy(d).wait_send()
+        m_copy(d).wait_send()
+        s4_copy(d).wait_send()
 
     def sent(q, carry):
         for j in range(4):
             if j == 0:
 
-                @pl.when(jnp.logical_not((q == m_own) & is_self))
+                @pl.when(jnp.logical_not(stays(q)))
                 def _():
                     return_copy(j, q).wait_send()
             else:
@@ -507,7 +616,7 @@
             pltpu.VMEM((BLK, 4 * F), bf16),
             pltpu.VMEM((BLK, 512), bf16),
             pltpu.VMEM((4, NQ, CAP, F), bf16),
-            pltpu.VMEM((64, CAP, F), bf16),
+            pltpu.VMEM((4, MEM, CAP, F), bf16),
             pltpu.VMEM((192, 4 * F), bf16),
             pltpu.VMEM((192, 4 * F), bf16),
             pltpu.VMEM((192, 1024), bf16),
@@ -515,6 +624,11 @@
             pltpu.VMEM((T, F), bf16),
             pltpu.VMEM((T, F), f32),
             pltpu.VMEM((8, T), f32),
+            pltpu.VMEM((4, 8, GT), f32),
+            pltpu.VMEM((4, 8, GT), f32),
+            pltpu.VMEM((4, GT, T), bf16),
+            pltpu.VMEM((4, GT, F), bf16),
+            pltpu.VMEM((4, GT, F), bf16),
             dma((8,)),
             dma((4,)), dma((4,)),
             dma((4,)), dma((4,)),
@@ -527,6 +641,8 @@
             dma((3,)), dma((3, 4)),
             dma((64,)), dma((64,)),
             dma((64,)), dma((64,)),
+            dma((4,)), dma((4,)),
+            dma((4,)), dma((4,)),
         ],
         compiler_params=pltpu.CompilerParams(collective_id=0, has_side_effects=True, vmem_limit_bytes=60 * 1024 * 1024),
         name="layer",

time: 194 us -> 178 us (0.918)
  the two profiles are of different devices: /device:TPU:32 before, /device:TPU:61 now
where the time goes in v3:
time: 178 us
  Pallas kernels  176 us (99%)
  local copies, waits for them, and re-layouts  2.06 us (1%)
    pallas_call x1, Pallas kernels, body(): pl.pallas_call(kernel, out_shape=jax.ShapeDtypeStruct((T, F), bf16), in_s...  176 us

profile of v3, /device:TPU:61, one launch (start us, length us, event | category | flops | bytes accessed | tf_op | source)
XLA Modules:
  0.0 178.0 jit_solution(11574197305348120930)
XLA Ops:
  0.0 175.9 %layer.1 = bf16[768,512]{1,0:T(8,128)(2,1)} custom-call(bf16[768,512]{1,0:T(8,128)(2,1)} %tok_hbm.1, f32[1,512]{1,0:T(1,128)} %bitcast.14, s32[2,768]{1,0:T(2,128)} %bitcast.12, f32[2,768]{1,0:T(2,128)} %bitcast.13, bf16[512,512]{1,0:T(8,128)(2,1)} %bitcast.8, bf16[512,512]{1,0:T(8,128)(2,1)} %bitcast.9, bf16[512,512]{1,0:T(8,128)(2,1)} %bitcast.10, ...), custom_call_target="tpu_custom_call" | custom-call | tf_op jit(solution)/shard_map/layer/pallas_call | solution.py:604
  176.0 2.1 %copy.12 = bf16[768,512]{1,0:T(8,128)(2,1)} copy(bf16[768,512]{1,0:T(8,128)(2,1)} %layer.1) | data formatting | bytes 1572864

commit v4 on v3

--- a/solution.py
+++ b/solution.py
@@ -14,7 +14,7 @@
 BLK = 4 * CAP
 GT = 384
 MEM = 16
-FIRST, SECOND = 3, 6
+FIRST, SECOND = 6, 12
 
 
 def kernel(
@@ -190,7 +190,6 @@
             dispatch_copy(q, j).start()
         return carry
 
-    lax.fori_loop(0, NQ, pack, 0)
     pl.semaphore_wait(barrier, 13 + 6 + 64 + 16 - 2 * is_self.astype(jnp.int32))
 
     mate = (x + 5 - 2 * rel) % 4
@@ -256,13 +255,17 @@
     for d in range(1, 4):
         gain_copy(d).start()
     w_start((0, 1))
-    lax.fori_loop(0, NQ, dispatch_straight, 0)
 
     @pl.when(primary)
     def _():
         for k in range(3):
             w_loads[k].wait()
             w_across(k, x).start()
+
+    def pack_and_send(q, carry):
+        return dispatch_straight(q, pack(q, carry))
+
+    lax.fori_loop(0, NQ, pack_and_send, 0)
 
     def w_relay(k):
         w_piece(k, outer, fsend.at[k], ep, x).wait_recv()
@@ -397,8 +400,8 @@
             else:
                 return_copy(jj, m).start()
 
-    def expert(i, carry):
-        part = (z // 2 + pair_at(i)) % 4
+    def hide(i, carry):
+        part = (z // 2 + jnp.where(i == 2, 3, jnp.where(i == 3, 2, i))) % 4
         for mm in range(4):
             m = part * 4 + mm
             for xx in range(4):
@@ -424,19 +427,15 @@
                     )
                 sums.append(total)
             gate_sum, up_sum = sums
-            hidden[:, cols] = (gate_sum / (1.0 + jnp.exp(-gate_sum)) * up_sum).astype(jnp.bfloat16)
-
-        @pl.when((i == 0) & primary)
-        def _():
-            w_last(2)
-
-        @pl.when((i == 0) & jnp.logical_not(primary))
-        def _():
-            w_served(2)
-
+            hidden[pl.ds(pl.multiple_of(part * BLK, BLK), BLK), cols] = (gate_sum / (1.0 + jnp.exp(-gate_sum)) * up_sum).astype(jnp.bfloat16)
+
+        return carry
+
+    def down(i, carry):
+        part = (z // 2 + pair_at(i)) % 4
         for jj in range(4):
             quarter = (x + (0, 1, 3, 2)[jj]) % 4
-            rows = jnp.dot(hidden[...], weights[2, quarter], preferred_element_type=jnp.float32)
+            rows = jnp.dot(hidden[pl.ds(pl.multiple_of(part * BLK, BLK), BLK), :], weights[2, quarter], preferred_element_type=jnp.float32)
             result[quarter, pl.ds(part * 4, 4)] = rows.astype(jnp.bfloat16).reshape(4, CAP, F)
 
             @pl.when(i < 3)
@@ -445,9 +444,19 @@
 
         return carry
 
-    lax.fori_loop(0, 4, expert, 0)
     for d in range(1, 4):
         btok_copy(d).start()
+    lax.fori_loop(0, 4, hide, 0)
+
+    @pl.when(primary)
+    def _():
+        w_last(2)
+
+    @pl.when(jnp.logical_not(primary))
+    def _():
+        w_served(2)
+
+    lax.fori_loop(0, 4, down, 0)
 
     def s4_copy(k):
         return remote(rq.at[k], back.at[group], s4send.at[k], s4recv.at[group], ep_of(source_z(k), y, c), x)
@@ -468,25 +477,24 @@
             rq[k] = total
             s4_copy(k).start()
 
+    for d in range(1, 4):
+        btok_copy(d).wait_recv()
+
+    def branch_norm(r, carry):
+        rows = pl.ds(pl.multiple_of(r * 16, 16), 16)
+        norm_rows(btok[rows, :], bnorm.at[rows, :])
+        return carry
+
+    lax.fori_loop(0, 12, branch_norm, 0)
+
+    relay(3)
+    for jj in range(4):
+        give_back(group, jj)
     for way in range(2):
         y_forward(way).wait_recv()
     for k in range(2):
         d_copy(k).start()
-    relay(3)
-    for jj in range(4):
-        give_back(group, jj)
     relay(2)
-    relay(1)
-    for d in range(1, 4):
-        btok_copy(d).wait_recv()
-
-    def branch_norm(r, carry):
-        rows = pl.ds(pl.multiple_of(r * 16, 16), 16)
-        norm_rows(btok[rows, :], bnorm.at[rows, :])
-        return carry
-
-    lax.fori_loop(0, 12, branch_norm, 0)
-
     for k in range(2):
         d_copy(k).wait_recv()
 
@@ -516,6 +524,7 @@
         else:
             bres[quarter] = rows.astype(jnp.bfloat16)
             bret_copy(d).start()
+    relay(1)
 
     for d in range(1, 8):
         z_copy(d).wait_send()
@@ -614,7 +623,7 @@
             pltpu.VMEM((3, 4, 512, 512), bf16),
             pltpu.VMEM((2, 8, 4, 2, 32, 1024), bf16),
             pltpu.VMEM((BLK, 4 * F), bf16),
-            pltpu.VMEM((BLK, 512), bf16),
+            pltpu.VMEM((T, 512), bf16),
             pltpu.VMEM((4, NQ, CAP, F), bf16),
             pltpu.VMEM((4, MEM, CAP, F), bf16),
             pltpu.VMEM((192, 4 * F), bf16),

time: 178 us -> 171 us (0.961)
  the two profiles are of different devices: /device:TPU:61 before, /device:TPU:32 now
where the time goes in v4:
time: 171 us
  Pallas kernels  169 us (99%)
  local copies, waits for them, and re-layouts  2.06 us (1%)
    pallas_call x1, Pallas kernels, body(): pl.pallas_call(kernel, out_shape=jax.ShapeDtypeStruct((T, F), bf16), in_s...  169 us

profile of v4, /device:TPU:32, one launch (start us, length us, event | category | flops | bytes accessed | tf_op | source)
XLA Modules:
  0.0 171.3 jit_solution(16720915858481217075)
XLA Ops:
  0.0 169.2 %layer.1 = bf16[768,512]{1,0:T(8,128)(2,1)} custom-call(bf16[768,512]{1,0:T(8,128)(2,1)} %tok_hbm.1, f32[1,512]{1,0:T(1,128)} %bitcast.14, s32[2,768]{1,0:T(2,128)} %bitcast.12, f32[2,768]{1,0:T(2,128)} %bitcast.13, bf16[512,512]{1,0:T(8,128)(2,1)} %bitcast.8, bf16[512,512]{1,0:T(8,128)(2,1)} %bitcast.9, bf16[512,512]{1,0:T(8,128)(2,1)} %bitcast.10, ...), custom_call_target="tpu_custom_call" | custom-call | tf_op jit(solution)/shard_map/layer/pallas_call | solution.py:613
  169.2 2.1 %copy.12 = bf16[768,512]{1,0:T(8,128)(2,1)} copy(bf16[768,512]{1,0:T(8,128)(2,1)} %layer.1) | data formatting | bytes 1572864

commit v5 on v4

--- a/solution.py
+++ b/solution.py
@@ -14,7 +14,7 @@
 BLK = 4 * CAP
 GT = 384
 MEM = 16
-FIRST, SECOND = 6, 12
+FIRST, SECOND = 6, 16
 
 
 def kernel(

time: 171 us -> 170 us (level); the launches traced: 171 us -> 168 us
  Pallas kernels: 169 us -> 166 us
    pallas_call x1, Pallas kernels: 169 us -> 166 us  [body(): pl.pallas_call(kernel, out_shape=jax.ShapeDtypeStruct((T, F), bf16), in_s...]
where the time goes in v5:
time: 170 us; the launch traced here: 168 us
  Pallas kernels  166 us (98%)
  local copies, waits for them, and re-layouts  2.06 us (1%)
    pallas_call x1, Pallas kernels, body(): pl.pallas_call(kernel, out_shape=jax.ShapeDtypeStruct((T, F), bf16), in_s...  166 us

profile of v5, /device:TPU:32, one launch (start us, length us, event | category | flops | bytes accessed | tf_op | source)
XLA Modules:
  0.0 167.8 jit_solution(16730845981961438206)
XLA Ops:
  0.0 165.7 %layer.1 = bf16[768,512]{1,0:T(8,128)(2,1)} custom-call(bf16[768,512]{1,0:T(8,128)(2,1)} %tok_hbm.1, f32[1,512]{1,0:T(1,128)} %bitcast.14, s32[2,768]{1,0:T(2,128)} %bitcast.12, f32[2,768]{1,0:T(2,128)} %bitcast.13, bf16[512,512]{1,0:T(8,128)(2,1)} %bitcast.8, bf16[512,512]{1,0:T(8,128)(2,1)} %bitcast.9, bf16[512,512]{1,0:T(8,128)(2,1)} %bitcast.10, ...), custom_call_target="tpu_custom_call" | custom-call | tf_op jit(solution)/shard_map/layer/pallas_call | solution.py:613
  165.7 2.1 %copy.12 = bf16[768,512]{1,0:T(8,128)(2,1)} copy(bf16[768,512]{1,0:T(8,128)(2,1)} %layer.1) | data formatting | bytes 1572864
